TPU v7x, 32 devices: a whole 2x2x4 slice. The times are simulated.
32 devices in a mesh: ep: 8 (over z, core), tp: 4 (over y, x).
Axes of the slice: x: 2, y: 2, z: 4, core: 2. Of those that a mesh axis runs over, the one named last changes fastest.
Arguments:
- tokens: bfloat16 [64, 2048], P('ep'), may hold values from -6 to 6
- attn_gain: float32 [2048], replicated, may hold values from 0.1 to 1.9
- query_weight: bfloat16 [2048, 4096], P('ep', 'tp'), may hold values from -0.125 to 0.125
- key_weight: bfloat16 [2048, 4096], P('ep', 'tp'), may hold values from -0.125 to 0.125
- value_weight: bfloat16 [2048, 4096], P('ep', 'tp'), may hold values from -0.125 to 0.125
- query_gain: float32 [128], replicated, may hold values from 0.1 to 1.9
- stick_bias: float32 [32], P('tp'), may hold values from -7 to -2.5
- key_cache: bfloat16 [64, 32, 512, 128], P('ep', 'tp'), may hold values from -6 to 6
- value_cache: bfloat16 [64, 32, 512, 128], P('ep', 'tp'), may hold values from -6 to 6
- lengths: int32 [64], P('ep'), may hold values from 64 to 512, as said below
- out_weight: bfloat16 [4096, 2048], P('tp'), may hold values from -0.375 to 0.375
- mix_gain: float32 [2048], replicated, may hold values from 0.1 to 1.9
- route_ids: int32 [64, 2], P('ep'), may hold values from 0 to 7, all different within a row; in each aligned block of 8 rows (0 to 7, 8 to 15, ...) at most 4 rows name the same one
- route_weights: float32 [64, 2], P('ep'), may hold values from 0.2 to 1
- expert_gate: bfloat16 [8, 2048, 2560], P('ep', None, 'tp'), may hold values from -0.125 to 0.125
- expert_up: bfloat16 [8, 2048, 2560], P('ep', None, 'tp'), may hold values from -0.125 to 0.125
- expert_down: bfloat16 [8, 2560, 2048], P('ep', 'tp'), may hold values from -0.15625 to 0.15625
- side_gate: bfloat16 [2048, 1024], P(None, 'tp'), may hold values from -0.125 to 0.125
- side_up: bfloat16 [2048, 1024], P(None, 'tp'), may hold values from -0.125 to 0.125
- side_down: bfloat16 [1024, 2048], P('tp'), may hold values from -0.25 to 0.25
- branch_gate: float32 [2048], replicated, may hold values from -0.125 to 0.125
Outputs:
- mixed: bfloat16 [64, 2048], P('ep', 'tp')
- new_keys: bfloat16 [64, 4096], P('ep', 'tp')
- new_values: bfloat16 [64, 4096], P('ep', 'tp')
Inputs may be any that keep to these rules, and one draw needn't show every extreme that they name: `lengths`: at least an eighth of 512; the first sequence has 512. `route_ids`: each token names 2 different experts. In the rows of one device no expert is named by more than 4 rows, a bound that some block reaches of some device.
All inputs are finite; a program needn't handle non-finite values.
Results may differ from a plain program's by a relative error of at most 0.018.
Values may be sent and summed in bfloat16 or wider, within the bound.
No kernel may reach another device: no remote copies, remote signals or barrier semaphores. Data moves between devices by JAX's collectives and lax.ppermute only.
A program may use at most 64 MiB of HBM per device.

v0:
```python
import jax
import jax.numpy as jnp
from jax import lax
from jax.sharding import PartitionSpec as P

DH = 128


epsilon = 1e-06


def rms_scale(values, scale_gain):
    mean_square = jnp.mean(values * values, axis=-1, keepdims=True)
    return values * lax.rsqrt(mean_square + epsilon) * scale_gain


def body(
    tokens,
    attn_gain,
    query_weight,
    key_weight,
    value_weight,
    query_gain,
    stick_bias,
    key_cache,
    value_cache,
    lengths,
    out_weight,
    mix_gain,
    route_ids,
    route_weights,
    expert_gate,
    expert_up,
    expert_down,
    side_gate,
    side_up,
    side_down,
    branch_gate,
):
    seq_count, model_width = tokens.shape
    head_cols = query_weight.shape[1]
    heads_local = key_cache.shape[1]
    cache_slots = key_cache.shape[2]
    stream = tokens.astype(jnp.float32)
    normed = rms_scale(stream, attn_gain).astype(jnp.bfloat16)
    stacked = jnp.concatenate([query_weight, key_weight, value_weight], axis=1)
    columns = lax.all_to_all(normed, "ep", split_axis=1, concat_axis=0, tiled=True)
    picked = columns
    projected = lax.psum_scatter(
        jnp.dot(picked, stacked, preferred_element_type=jnp.float32),
        "ep",
        scatter_dimension=0,
        tiled=True,
    )
    query_rows = projected[:, :head_cols].astype(jnp.bfloat16)
    fresh_keys = projected[:, head_cols : 2 * head_cols].astype(jnp.bfloat16)
    new_values = projected[:, 2 * head_cols :].astype(jnp.bfloat16)
    new_keys = rms_scale(fresh_keys.astype(jnp.float32).reshape(seq_count, heads_local, DH), 1.0)
    new_keys = new_keys.astype(jnp.bfloat16).reshape(seq_count, head_cols)
    query_heads = rms_scale(
        query_rows.astype(jnp.float32).reshape(seq_count, heads_local, DH), query_gain
    )
    query_heads = query_heads.astype(jnp.bfloat16)
    scores = jnp.einsum("shd,shld->shl", query_heads, key_cache, preferred_element_type=jnp.float32)
    scores = scores * DH ** (-0.5) + stick_bias[None, :, None]
    positions = jnp.arange(cache_slots, dtype=jnp.int32)
    visible = positions[None, None, :] < lengths[:, None, None]
    log_rest = jnp.where(visible, jax.nn.log_sigmoid(-scores), 0.0)
    log_between = lax.cumsum(log_rest, axis=2, reverse=True) - log_rest
    stick = jnp.where(visible, jnp.exp(jax.nn.log_sigmoid(scores) + log_between), 0.0).astype(
        jnp.bfloat16
    )
    attended = jnp.einsum("shl,shld->shd", stick, value_cache, preferred_element_type=jnp.float32)
    attended = attended.astype(jnp.bfloat16).reshape(seq_count, head_cols)
    attn_proj = lax.psum(
        jnp.dot(attended, out_weight, preferred_element_type=jnp.float32).astype(jnp.bfloat16), "tp"
    ).astype(jnp.float32)
    middle = (stream + attn_proj).astype(jnp.bfloat16)
    normed_mix = rms_scale(middle.astype(jnp.float32), mix_gain).astype(jnp.bfloat16)
    side_gate_pre = jnp.dot(normed_mix, side_gate, preferred_element_type=jnp.float32)
    side_up_pre = jnp.dot(normed_mix, side_up, preferred_element_type=jnp.float32)
    side_hidden = (jax.nn.silu(side_gate_pre) * side_up_pre).astype(jnp.bfloat16)
    side_term = jnp.dot(side_hidden, side_down, preferred_element_type=jnp.float32)
    switch = jax.nn.sigmoid(
        jnp.sum(normed_mix.astype(jnp.float32) * branch_gate, axis=1, keepdims=True)
    )
    experts = lax.axis_size("ep")
    top_count = route_ids.shape[1]
    capacity = max(2, 2 * top_count * seq_count // experts)
    flat_ids = route_ids.reshape(-1)
    onehot = (flat_ids[:, None] == jnp.arange(experts, dtype=jnp.int32)[None, :]).astype(jnp.int32)
    before = jnp.cumsum(onehot, axis=0) - onehot
    slot_index = jnp.sum(before * onehot, axis=1)
    target = flat_ids * capacity + slot_index
    route_map = (
        target[:, None] == jnp.arange(experts * capacity, dtype=jnp.int32)[None, :]
    ).astype(jnp.bfloat16)
    dispatch = jnp.sum(route_map.reshape(seq_count, top_count, experts * capacity), axis=1).T
    outbox = jnp.dot(dispatch, normed_mix, preferred_element_type=jnp.float32).astype(jnp.bfloat16)
    outbox = outbox.reshape(experts, capacity, model_width)
    col_width = model_width // lax.axis_size("tp")
    col_offset = lax.axis_index("tp") * col_width
    arrived = lax.all_to_all(outbox, "ep", split_axis=0, concat_axis=0, tiled=True)
    slot_rows = arrived.reshape(experts * capacity, model_width)
    gate_pre = jnp.dot(slot_rows, expert_gate[0], preferred_element_type=jnp.float32)
    up_pre = jnp.dot(slot_rows, expert_up[0], preferred_element_type=jnp.float32)
    hidden = (jax.nn.silu(gate_pre) * up_pre).astype(jnp.bfloat16)
    expert_term = jnp.dot(hidden, expert_down[0], preferred_element_type=jnp.float32)
    expert_part, side_part = (
        lax.psum_scatter(
            expert_term.astype(jnp.bfloat16), "tp", scatter_dimension=1, tiled=True
        ).astype(jnp.float32),
        lax.psum_scatter(
            side_term.astype(jnp.bfloat16), "tp", scatter_dimension=1, tiled=True
        ).astype(jnp.float32),
    )
    returned = lax.all_to_all(
        expert_part.astype(jnp.bfloat16).reshape(experts, capacity, col_width),
        "ep",
        split_axis=0,
        concat_axis=0,
        tiled=True,
    )
    picked = jnp.dot(
        route_map,
        returned.reshape(experts * capacity, col_width),
        preferred_element_type=jnp.float32,
    )
    routed = jnp.sum(
        route_weights[:, :, None] * picked.reshape(seq_count, top_count, col_width), axis=1
    )
    middle_cols = lax.dynamic_slice_in_dim(middle, col_offset, col_width, 1).astype(jnp.float32)
    mixed = (middle_cols + routed + switch * side_part).astype(jnp.bfloat16)
    return (mixed, new_keys, new_values)


def solution(mesh):
    in_specs = (
        P("ep", None),
        P(),
        P("ep", "tp"),
        P("ep", "tp"),
        P("ep", "tp"),
        P(),
        P("tp"),
        P("ep", "tp", None, None),
        P("ep", "tp", None, None),
        P("ep"),
        P("tp", None),
        P(),
        P("ep", None),
        P("ep", None),
        P("ep", None, "tp"),
        P("ep", None, "tp"),
        P("ep", "tp", None),
        P(None, "tp"),
        P(None, "tp"),
        P("tp", None),
        P(),
    )
    out_specs = (P("ep", "tp"), P("ep", "tp"), P("ep", "tp"))
    return jax.shard_map(body, mesh=mesh, in_specs=in_specs, out_specs=out_specs, check_vma=False)
```

profile of v0, /device:TPU:0, one launch (start us, length us, event | category | flops | bytes accessed | tf_op | source)
XLA Modules:
  0.0 196.1 jit_solution(3717251648128114793)
XLA Ops:
  7.2 0.0 copy-start
  7.2 0.0 copy-start.6
  7.2 0.0 copy-start.8
  7.2 0.0 copy-start.7
  7.2 0.0 reduce-scatter.4.cloned.1.call-start
  7.3 1.0 fusion.44
  8.3 0.8 fusion.46
  9.1 11.9 %all_to_all.29 = bf16[8,8,256]{2,0,1:T(8,128)(2,1)S(1)} all-to-all(bf16[8,8,256]{2,0,1:T(8,128)(2,1)S(1)} %bitcast.88), channel_id=1, replica_groups=mesh['ep'=8,'tp'=4] {'ep'}, dimensions={1} | all-to-all | bytes 65536 | tf_op jit(solution)/shard_map/all_to_all | solution.py:47
  21.0 2.6 %fusion.9 = f32[64,3072]{1,0:T(8,128)} fusion(bf16[256,1024]{1,0:T(8,128)(2,1)} %param.25, bf16[256,1024]{1,0:T(8,128)(2,1)} %param.24, bf16[256,1024]{1,0:T(8,128)(2,1)} %param.23, bf16[8,8,256]{2,0,1:T(8,128)(2,1)S(1)} %all_to_all.29), kind=kOutput, calls=%fused_computation.10 | convolution fusion | flops 105381888 | bytes 2392064 | tf_op jit(solution)/shard_map/dot_general | solution.py:50
  23.7 0.0 reduce-scatter.4.cloned.1.call-update
  23.7 0.0 copy-done.6
  23.7 0.1 copy.34
  23.8 0.1 eq.51
  23.9 0.1 fusion.69
  24.0 0.2 select_reduce_fusion
  24.2 0.1 reduce_sum.80
  24.2 0.1 copy.36
  24.3 0.1 fusion.73
  24.4 0.0 copy-done.8
  24.4 0.1 iota_compare_fusion
  24.5 29.5 %reduce-scatter.4.cloned.1.call-done = f32[8,3072]{1,0:T(8,128)} async-done(((f32[64,3072]{1,0:T(8,128)}), f32[8,3072]{1,0:T(8,128)}) %reduce-scatter.4.cloned.1.call-update) | async-done | bytes 98320 | tf_op jit(solution)/shard_map/reduce_scatter | solution.py:49
  54.0 0.9 convert.7
  54.9 0.1 fusion.51
  55.0 0.0 copy-done.7
  55.0 0.1 fusion.59
  55.1 5.7 %fusion.57 = f32[8,8,1,512]{3,2,1,0:T(1,128)S(1)} fusion(bf16[8,8,512,128]{3,2,1,0:T(8,128)(2,1)} %param.28, bf16[8,8,128,1]{2,0,1,3:T(8,128)(2,1)S(1)} %fusion.59), kind=kOutput, calls=%fused_computation.68 | convolution fusion | flops 8388608 | bytes 8536064 | tf_op jit(solution)/shard_map/shd,shld->shl/dot_general | solution.py:64
  60.8 0.0 copy-done.5
  60.8 0.2 fusion.35
  61.0 39.6 %reduce-window.6 = f32[8,8,4,128]{3,1,2,0:T(8,128)S(1)} reduce-window(f32[8,8,4,128]{3,1,2,0:T(8,128)S(1)} %fusion.35, f32[]{:T(128)} %constant.17.clone.1), window={size=1x1x1x128 pad=0_0x0_0x0_0x0_127}, to_apply=%region_3.0 | reduce-window | flops 4161536 | bytes 262148 | tf_op jit(solution)/shard_map/reduce-window
  100.6 0.2 copy.32
  100.8 0.1 fusion.62
  101.0 0.3 fusion.48
  101.3 0.0 copy-start.1
  101.3 4.7 %fusion.33 = f32[8,8,1,128]{3,2,1,0:T(1,128)S(1)} fusion(bf16[8,8,512,128]{3,2,1,0:T(8,128)(2,1)} %param.29, bf16[8,8,512,1]{2,1,0,3:T(8,128)(2,1)S(1)} %fusion.48), kind=kOutput, calls=%fused_computation.34 | convolution fusion | flops 8388608 | bytes 8486912 | tf_op jit(solution)/shard_map/shl,shld->shd/dot_general | solution.py:73
  106.0 0.0 copy-start.4
  106.1 0.7 convolution_convert_fusion.2
  106.7 16.2 %psum.7 = bf16[8,2048]{1,0:T(8,128)(2,1)S(1)} all-reduce(bf16[8,2048]{1,0:T(8,128)(2,1)S(1)} %convolution_convert_fusion.2), channel_id=1, replica_groups=mesh['ep'=8,'tp'=4] {'tp'}, use_global_device_ids=true, to_apply=%region_5.6 | all-reduce | flops 16384 | bytes 65536 | tf_op jit(solution)/shard_map/psum | solution.py:75
  123.0 0.0 copy-done.2
  123.0 0.1 fusion.41
  123.1 0.2 convolution_convert_fusion
  123.4 0.7 reshape.161
  124.1 3.4 %all-to-all-start.1 = ((bf16[8,4,2048]{2,1,0:T(4,128)(2,1)}), bf16[8,4,2048]{2,1,0:T(4,128)(2,1)S(1)}, u32[]{:S(2)}, u32[]{:S(2)}) async-start(bf16[8,4,2048]{2,1,0:T(4,128)(2,1)} %reshape.161), calls=%async_computation.2 | async-start | bytes 262144 | tf_op jit(solution)/shard_map/all_to_all | solution.py:103
  127.4 0.0 reduce-scatter.6.cloned.1.call-start
  127.5 1.5 fusion.81
  129.0 0.0 copy-done.4
  129.0 0.2 multiply_reduce_fusion
  129.2 0.6 slice.27
  129.8 0.7 fusion.52
  130.5 3.6 %all-to-all-done.1 = bf16[8,4,2048]{2,1,0:T(4,128)(2,1)S(1)} async-done(((bf16[8,4,2048]{2,1,0:T(4,128)(2,1)}), bf16[8,4,2048]{2,1,0:T(4,128)(2,1)S(1)}, u32[]{:S(2)}, u32[]{:S(2)}) %all-to-all-start.1) | async-done | bytes 131104 | tf_op jit(solution)/shard_map/all_to_all | solution.py:103
  134.2 2.3 %fusion.4 = f32[32,640]{1,0:T(8,128)S(1)} fusion(bf16[32,2048]{1,0:T(8,128)(2,1)S(1)} %reshape.162, bf16[1,2048,640]{2,1,0:T(8,128)(2,1)} %param.35), kind=kOutput, calls=%fused_computation.4 | convolution fusion | flops 83886080 | bytes 2834432 | tf_op jit(solution)/shard_map/dot_general | solution.py:105
  136.4 0.0 copy-start.9
  136.5 3.4 %fusion.6 = bf16[32,2048]{1,0:T(8,128)(2,1)} fusion(bf16[1,640,2048]{2,1,0:T(8,128)(2,1)S(1)} %copy-done, bf16[32,2048]{1,0:T(8,128)(2,1)S(1)} %reshape.162, bf16[1,2048,640]{2,1,0:T(8,128)(2,1)} %param.36, f32[32,640]{1,0:T(8,128)S(1)} %fusion.4), kind=kOutput, calls=%fused_computation.6 | convolution fusion | flops 167960576 | bytes 5586944 | tf_op jit(solution)/shard_map/dot_general | solution.py:108
  139.8 0.0 reduce-scatter.6.cloned.1.call-update
  139.9 0.0 reduce-scatter.8.cloned.1.call-start
  139.9 2.9 %convolution_convert_fusion.1 = bf16[8,2048]{1,0:T(8,128)(2,1)} fusion(bf16[256,2048]{1,0:T(8,128)(2,1)} %param.40, bf16[2048,256]{1,0:T(8,128)(2,1)} %param.39, f32[8,256]{1,0:T(8,128)S(1)} %fusion.81, bf16[8,2048]{1,0:T(8,128)(2,1)S(1)} %get-tuple-element.6, f32[2048]{0:T(1024)S(1)} %copy-done.3, f32[8]{0:T(128)S(1)} %add_rsqrt_fusion.2), kind=kOutput, calls=%fused_computation.8 | convolution fusion | flops 16871424 | bytes 2179104 | tf_op jit(solution)/shard_map/dot_general | solution.py:83
  142.8 0.0 reduce-scatter.8.cloned.1.call-update
  142.8 18.5 %reduce-scatter.6.cloned.1.call-done = bf16[32,512]{1,0:T(8,128)(2,1)} async-done(((bf16[32,2048]{1,0:T(8,128)(2,1)}), bf16[32,512]{1,0:T(8,128)(2,1)}) %reduce-scatter.6.cloned.1.call-update) | async-done | bytes 32784 | tf_op jit(solution)/shard_map/reduce_scatter | solution.py:110
  161.4 1.4 reshape.163
  162.7 4.6 %all-to-all-start.2 = ((bf16[8,4,512]{2,1,0:T(4,128)(2,1)}), bf16[8,4,512]{2,1,0:T(4,128)(2,1)S(1)}, u32[]{:S(2)}, u32[]{:S(2)}) async-start(bf16[8,4,512]{2,1,0:T(4,128)(2,1)} %reshape.163), calls=%async_computation.4 | async-start | bytes 65536 | tf_op jit(solution)/shard_map/all_to_all | solution.py:117
  167.3 5.7 %all-to-all-done.2 = bf16[8,4,512]{2,1,0:T(4,128)(2,1)S(1)} async-done(((bf16[8,4,512]{2,1,0:T(4,128)(2,1)}), bf16[8,4,512]{2,1,0:T(4,128)(2,1)S(1)}, u32[]{:S(2)}, u32[]{:S(2)}) %all-to-all-start.2) | async-done | bytes 32800 | tf_op jit(solution)/shard_map/all_to_all | solution.py:117
  173.1 0.0 copy-done.9
  173.1 0.2 fusion.21
  173.3 14.9 %reduce-scatter.8.cloned.1.call-done = bf16[8,512]{1,0:T(8,128)(2,1)} async-done(((bf16[8,2048]{1,0:T(8,128)(2,1)}), bf16[8,512]{1,0:T(8,128)(2,1)}) %reduce-scatter.8.cloned.1.call-update) | async-done | bytes 8208 | tf_op jit(solution)/shard_map/reduce_scatter | solution.py:113
  188.2 1.4 add_convert_fusion
  (18 shorter events, 0.1 us)
Async XLA Ops:
  7.2 129.3 %copy-start = (bf16[1,640,2048]{2,1,0:T(8,128)(2,1)S(1)}, bf16[1,640,2048]{2,1,0:T(8,128)(2,1)}, u32[]{:S(2)}) copy-start(bf16[1,640,2048]{2,1,0:T(8,128)(2,1)} %param.37) | copy-start | bytes 7864324
  7.2 16.5 %copy-start.6 = (s32[8,2]{0,1:T(2,128)S(1)}, s32[8,2]{0,1:T(2,128)}, u32[]{:S(2)}) copy-start(s32[8,2]{0,1:T(2,128)} %param.33) | copy-start | bytes 196
  7.2 17.2 %copy-start.8 = (s32[8]{0:T(128)S(1)}, s32[8]{0:T(128)}, u32[]{:S(2)}) copy-start(s32[8]{0:T(128)} %param.30) | copy-start | bytes 100
  7.2 47.8 %copy-start.7 = (f32[128]{0:T(128)S(1)}, f32[128]{0:T(128)}, u32[]{:S(2)}) copy-start(f32[128]{0:T(128)} %param.26) | copy-start | bytes 1540
  7.2 46.8 %reduce-scatter.4.cloned.1.call-start = ((), (), s32[]{:S(2)}) async-start(), calls=%async_computation.6 | async-start | bytes 884736 | tf_op jit(solution)/shard_map/reduce_scatter | solution.py:49
  55.1 5.7 %copy-start.5 = (f32[8]{0:T(128)S(1)}, f32[8]{0:T(128)}, u32[]{:S(2)}) copy-start(f32[8]{0:T(128)} %param.27) | copy-start | bytes 100
  101.3 4.8 %copy-start.1 = (bf16[1024,2048]{1,0:T(8,128)(2,1)S(1)}, bf16[1024,2048]{1,0:T(8,128)(2,1)}, u32[]{:S(2)}) copy-start(bf16[1024,2048]{1,0:T(8,128)(2,1)} %param.31) | copy-start | bytes 12582916
  106.0 17.0 %copy-start.2 = (bf16[8,2048]{1,0:T(8,128)(2,1)S(1)}, bf16[8,2048]{1,0:T(8,128)(2,1)}, u32[]{:S(2)}) copy-start(bf16[8,2048]{1,0:T(8,128)(2,1)} %param.21) | copy-start | bytes 98308
  106.0 17.1 %copy-start.3 = (f32[2048]{0:T(1024)S(1)}, f32[2048]{0:T(1024)}, u32[]{:S(2)}) copy-start(f32[2048]{0:T(1024)} %param.32) | copy-start | bytes 24580
  106.0 23.0 %copy-start.4 = (f32[2048]{0:T(1024)S(1)}, f32[2048]{0:T(1024)}, u32[]{:S(2)}) copy-start(f32[2048]{0:T(1024)} %param.41) | copy-start | bytes 24580
  124.1 10.1 %all-to-all-start.1 = ((bf16[8,4,2048]{2,1,0:T(4,128)(2,1)}), bf16[8,4,2048]{2,1,0:T(4,128)(2,1)S(1)}, u32[]{:S(2)}, u32[]{:S(2)}) async-start(bf16[8,4,2048]{2,1,0:T(4,128)(2,1)} %reshape.161), calls=%async_computation.2 | async-start | bytes 262144 | tf_op jit(solution)/shard_map/all_to_all | solution.py:103
  127.4 33.9 %reduce-scatter.6.cloned.1.call-start = ((), (), s32[]{:S(2)}) async-start(), calls=%async_computation.7 | async-start | bytes 163840 | tf_op jit(solution)/shard_map/reduce_scatter | solution.py:110
  136.4 36.7 %copy-start.9 = (f32[8,2]{0,1:T(2,128)S(1)}, f32[8,2]{0,1:T(2,128)}, u32[]{:S(2)}) copy-start(f32[8,2]{0,1:T(2,128)} %param.34) | copy-start | bytes 196
  139.9 48.3 %reduce-scatter.8.cloned.1.call-start = ((), (), s32[]{:S(2)}) async-start(), calls=%async_computation.8 | async-start | bytes 40960 | tf_op jit(solution)/shard_map/reduce_scatter | solution.py:113
  162.7 10.4 %all-to-all-start.2 = ((bf16[8,4,512]{2,1,0:T(4,128)(2,1)}), bf16[8,4,512]{2,1,0:T(4,128)(2,1)S(1)}, u32[]{:S(2)}, u32[]{:S(2)}) async-start(bf16[8,4,512]{2,1,0:T(4,128)(2,1)} %reshape.163), calls=%async_computation.4 | async-start | bytes 65536 | tf_op jit(solution)/shard_map/all_to_all | solution.py:117
Sparse Core Ops, SparseCore 0:
  23.8 30.1 reduce-scatter.3
  140.0 21.3 reduce-scatter.5
  164.1 24.0 reduce-scatter.7
where the time goes:
time: 197 us; the launch traced here: 196 us
  waiting for transfers between devices  72.3 us (37%)
  other arithmetic  46 us (23%)
  blocking collectives  28.1 us (14%)
  matrix products  24.1 us (12%)
  between operations  14 us (7%)
  starting transfers between devices  8.11 us (4%)
  local copies, waits for them, and re-layouts  3.37 us (2%)
    another operation x3, other arithmetic  40.6 us
    reduce_scatter x1, waiting for transfers between devices, body(): lax.psum_scatter(jnp.dot(picked, stacked, preferred_element_type=jnp.floa...  29.5 us
    reduce_scatter x1, waiting for transfers between devices, body(): lax.psum_scatter(expert_term.astype(jnp.bfloat16), 'tp', scatter_dimensio...  18.5 us
    psum x1, blocking collectives, body(): lax.psum(jnp.dot(attended, out_weight, preferred_element_type=jnp.float32...  16.2 us
    reduce_scatter x1, waiting for transfers between devices, body(): lax.psum_scatter(side_term.astype(jnp.bfloat16), 'tp', scatter_dimension=...  14.9 us
    all_to_all x1, blocking collectives, body(): lax.all_to_all(normed, 'ep', split_axis=1, concat_axis=0, tiled=True)  11.9 us
    all_to_all x1, waiting for transfers between devices, body(): lax.all_to_all(expert_part.astype(jnp.bfloat16).reshape(experts, capacity...  5.73 us
    dot_general x1, matrix products, body(): jnp.einsum('shd,shld->shl', query_heads, key_cache, preferred_element_typ...  5.65 us
  transfers between devices with their start and end apart: 5, of which 5 were waited for; matrix products, arithmetic and copies ran while one was open for 4% of the time, Pallas kernels for 0%

commit v1 on v0

v1 whole, which is shorter than its diff:
```python
import jax
import jax.numpy as jnp
from jax import lax
from jax.sharding import PartitionSpec as P

DH = 128


epsilon = 1e-06


def rms_scale(values, scale_gain):
    mean_square = jnp.mean(values * values, axis=-1, keepdims=True)
    return values * lax.rsqrt(mean_square + epsilon) * scale_gain


def summed_blocks(partial, axis_name):
    count = lax.axis_size(axis_name)
    rows = partial.shape[0] // count
    blocks = lax.all_to_all(
        partial.astype(jnp.bfloat16), axis_name, split_axis=0, concat_axis=0, tiled=True
    )
    return jnp.sum(blocks.reshape(count, rows, -1).astype(jnp.float32), axis=0)


def body(
    tokens,
    attn_gain,
    query_weight,
    key_weight,
    value_weight,
    query_gain,
    stick_bias,
    key_cache,
    value_cache,
    lengths,
    out_weight,
    mix_gain,
    route_ids,
    route_weights,
    expert_gate,
    expert_up,
    expert_down,
    side_gate,
    side_up,
    side_down,
    branch_gate,
):
    seq_count, model_width = tokens.shape
    head_cols = query_weight.shape[1]
    heads_local = key_cache.shape[1]
    cache_slots = key_cache.shape[2]
    experts = lax.axis_size("ep")
    tp_size = lax.axis_size("tp")
    stream = tokens.astype(jnp.float32)
    normed = rms_scale(stream, attn_gain).astype(jnp.bfloat16)
    columns = lax.all_to_all(normed, "ep", split_axis=1, concat_axis=0, tiled=True)
    query_rows = summed_blocks(
        jnp.dot(columns, query_weight, preferred_element_type=jnp.float32), "ep"
    ).astype(jnp.bfloat16)
    query_heads = rms_scale(
        query_rows.astype(jnp.float32).reshape(seq_count, heads_local, DH), query_gain
    ).astype(jnp.bfloat16)
    fresh = jnp.concatenate(
        [
            jnp.dot(columns, key_weight, preferred_element_type=jnp.float32),
            jnp.dot(columns, value_weight, preferred_element_type=jnp.float32),
        ],
        axis=1,
    )
    fresh = summed_blocks(fresh, "ep").astype(jnp.bfloat16)
    new_values = fresh[:, head_cols:]
    new_keys = rms_scale(
        fresh[:, :head_cols].astype(jnp.float32).reshape(seq_count, heads_local, DH), 1.0
    )
    new_keys = new_keys.astype(jnp.bfloat16).reshape(seq_count, head_cols)

    scores = jnp.einsum("shd,shld->shl", query_heads, key_cache, preferred_element_type=jnp.float32)
    scores = scores * DH ** (-0.5) + stick_bias[None, :, None]
    positions = jnp.arange(cache_slots, dtype=jnp.int32)
    visible = positions[None, None, :] < lengths[:, None, None]
    log_rest = jnp.where(visible, jax.nn.log_sigmoid(-scores), 0.0)
    later = (positions[:, None] > positions[None, :]).astype(jnp.float32)
    log_between = jnp.dot(
        log_rest.reshape(-1, cache_slots), later, precision=lax.Precision.HIGHEST
    ).reshape(scores.shape)
    stick = jnp.where(visible, jnp.exp(jax.nn.log_sigmoid(scores) + log_between), 0.0).astype(
        jnp.bfloat16
    )
    attended = jnp.einsum("shl,shld->shd", stick, value_cache, preferred_element_type=jnp.float32)
    attended = attended.astype(jnp.bfloat16).reshape(seq_count, head_cols)
    attn_part = jnp.dot(attended, out_weight, preferred_element_type=jnp.float32)
    attn_parts = lax.all_gather(attn_part.astype(jnp.bfloat16), "tp", axis=0, tiled=False)
    attn_proj = jnp.sum(attn_parts.astype(jnp.float32), axis=0)
    middle = (stream + attn_proj).astype(jnp.bfloat16)
    normed_mix = rms_scale(middle.astype(jnp.float32), mix_gain).astype(jnp.bfloat16)

    top_count = route_ids.shape[1]
    capacity = max(2, 2 * top_count * seq_count // experts)
    slots = experts * capacity
    flat_ids = route_ids.reshape(-1)
    onehot = (flat_ids[:, None] == jnp.arange(experts, dtype=jnp.int32)[None, :]).astype(jnp.int32)
    order = jnp.arange(flat_ids.shape[0], dtype=jnp.int32)
    earlier = (order[:, None] > order[None, :]) & (flat_ids[:, None] == flat_ids[None, :])
    slot_index = jnp.sum(earlier.astype(jnp.int32), axis=1)
    target = flat_ids * capacity + slot_index
    route_map = (target[:, None] == jnp.arange(slots, dtype=jnp.int32)[None, :]).astype(
        jnp.bfloat16
    )
    dispatch = jnp.sum(route_map.reshape(seq_count, top_count, slots), axis=1).T
    outbox = jnp.dot(dispatch, normed_mix, preferred_element_type=jnp.float32).astype(jnp.bfloat16)
    slot_rows = lax.all_to_all(outbox, "ep", split_axis=0, concat_axis=0, tiled=True)

    side_gate_pre = jnp.dot(normed_mix, side_gate, preferred_element_type=jnp.float32)
    side_up_pre = jnp.dot(normed_mix, side_up, preferred_element_type=jnp.float32)
    side_hidden = (jax.nn.silu(side_gate_pre) * side_up_pre).astype(jnp.bfloat16)
    side_term = jnp.dot(side_hidden, side_down, preferred_element_type=jnp.float32)
    switch = jax.nn.sigmoid(
        jnp.sum(normed_mix.astype(jnp.float32) * branch_gate, axis=1, keepdims=True)
    )
    col_width = model_width // tp_size
    col_offset = lax.axis_index("tp") * col_width
    side_blocks = lax.all_to_all(
        side_term.astype(jnp.bfloat16).reshape(seq_count, tp_size, col_width).transpose(1, 0, 2),
        "tp",
        split_axis=0,
        concat_axis=0,
        tiled=True,
    )
    side_part = jnp.sum(side_blocks.astype(jnp.float32), axis=0)

    gate_pre = jnp.dot(slot_rows, expert_gate[0], preferred_element_type=jnp.float32)
    up_pre = jnp.dot(slot_rows, expert_up[0], preferred_element_type=jnp.float32)
    hidden = (jax.nn.silu(gate_pre) * up_pre).astype(jnp.bfloat16)
    expert_term = jnp.dot(hidden, expert_down[0], preferred_element_type=jnp.float32)
    expert_term = expert_term.astype(jnp.bfloat16).reshape(experts, capacity, tp_size, col_width)
    returned = lax.all_to_all(
        expert_term.transpose(0, 2, 1, 3).reshape(experts * tp_size, capacity, col_width),
        ("ep", "tp"),
        split_axis=0,
        concat_axis=0,
        tiled=True,
    )
    expert_out = jnp.sum(
        returned.reshape(experts, tp_size, capacity, col_width).astype(jnp.float32), axis=1
    ).astype(jnp.bfloat16)
    picked = jnp.dot(
        route_map, expert_out.reshape(slots, col_width), preferred_element_type=jnp.float32
    )
    routed = jnp.sum(
        route_weights[:, :, None] * picked.reshape(seq_count, top_count, col_width), axis=1
    )
    middle_cols = lax.dynamic_slice_in_dim(middle, col_offset, col_width, 1).astype(jnp.float32)
    mixed = (middle_cols + routed + switch * side_part).astype(jnp.bfloat16)
    return (mixed, new_keys, new_values)


def solution(mesh):
    in_specs = (
        P("ep", None),
        P(),
        P("ep", "tp"),
        P("ep", "tp"),
        P("ep", "tp"),
        P(),
        P("tp"),
        P("ep", "tp", None, None),
        P("ep", "tp", None, None),
        P("ep"),
        P("tp", None),
        P(),
        P("ep", None),
        P("ep", None),
        P("ep", None, "tp"),
        P("ep", None, "tp"),
        P("ep", "tp", None),
        P(None, "tp"),
        P(None, "tp"),
        P("tp", None),
        P(),
    )
    out_specs = (P("ep", "tp"), P("ep", "tp"), P("ep", "tp"))
    return jax.shard_map(body, mesh=mesh, in_specs=in_specs, out_specs=out_specs, check_vma=False)
```

time: 197 us -> 92.9 us (0.47)
  waiting for transfers between devices: 72.3 us -> 28.4 us
  other arithmetic: 46 us -> 6.32 us
  blocking collectives: 28.1 us -> 8.59 us
  starting transfers between devices: 8.11 us -> 22.3 us
  between operations: 14 us -> 0.89 us
  matrix products: 24.1 us -> 21.2 us
    reduce_scatter x3 -> x0, waiting for transfers between devices: 62.9 us -> none  [the longest x1 29.5 us: body(): lax.psum_scatter(jnp.dot(picked, stacked, preferred_element_type=jnp.floa...]
    another operation x4 -> x0, other arithmetic: 40.7 us -> none
    psum x1 -> x0, blocking collectives: 16.2 us -> none  [body(): lax.psum(jnp.dot(attended, out_weight, preferred_element_type=jnp.float32...]
    all_to_all x1 -> x5, waiting for transfers between devices: 5.73 us -> 21.7 us  [the longest x2 7.22 us: summed_blocks(): lax.all_to_all(partial.astype(jnp.bfloat16), axis_name, split_axis=0, con...]
    all_to_all x1 -> x5, starting transfers between devices: 4.61 us -> 19 us  [the longest x2 6.78 us: summed_blocks(): lax.all_to_all(partial.astype(jnp.bfloat16), axis_name, split_axis=0, con...]
    all_to_all x1 -> x0, blocking collectives: 11.9 us -> none  [body(): lax.all_to_all(normed, 'ep', split_axis=1, concat_axis=0, tiled=True)]
    all_gather x0 -> x1, blocking collectives: none -> 8.59 us  [body(): lax.all_gather(attn_part.astype(jnp.bfloat16), 'tp', axis=0, tiled=False)]
    dot_general x1, matrix products: 4.73 us -> 1.19 us  [body(): jnp.einsum('shl,shld->shd', stick, value_cache, preferred_element_type=jn...]
  transfers between devices with their start and end apart: 5 -> 6, of which waited for: 5 -> 6; matrix products, arithmetic and copies ran while one was open for 4% -> 14% of each run, Pallas kernels for 0% -> 0%
where the time goes in v1:
time: 92.9 us; the launch traced here: 91.9 us
  waiting for transfers between devices  28.4 us (31%)
  starting transfers between devices  22.3 us (24%)
  matrix products  21.2 us (23%)
  blocking collectives  8.59 us (9%)
  other arithmetic  6.32 us (7%)
  local copies, waits for them, and re-layouts  4.18 us (4%)
    all_gather x1, blocking collectives, body(): lax.all_gather(attn_part.astype(jnp.bfloat16), 'tp', axis=0, tiled=False)  8.59 us
    all_to_all x2, waiting for transfers between devices, summed_blocks(): lax.all_to_all(partial.astype(jnp.bfloat16), axis_name, split_axis=0, con...  7.22 us
    all_to_all x1, waiting for transfers between devices, body(): lax.all_to_all(expert_term.transpose(0, 2, 1, 3).reshape(experts * tp_siz...  6.94 us
    all_to_all x2, starting transfers between devices, summed_blocks(): lax.all_to_all(partial.astype(jnp.bfloat16), axis_name, split_axis=0, con...  6.78 us
    all_to_all x1, waiting for transfers between devices, body(): lax.all_to_all(outbox, 'ep', split_axis=0, concat_axis=0, tiled=True)  6.65 us
    all_to_all x1, starting transfers between devices, body(): lax.all_to_all(normed, 'ep', split_axis=1, concat_axis=0, tiled=True)  6.35 us
    dot_general x1, matrix products, body(): jnp.einsum('shd,shld->shl', query_heads, key_cache, preferred_element_typ...  5.79 us
    all_to_all x1, waiting for transfers between devices, body(): lax.all_to_all(side_term.astype(jnp.bfloat16).reshape(seq_count, tp_size,...  3.8 us
  transfers between devices with their start and end apart: 6, of which 6 were waited for; matrix products, arithmetic and copies ran while one was open for 14% of the time, Pallas kernels for 0%

profile of v1, /device:TPU:0, one launch (start us, length us, event | category | flops | bytes accessed | tf_op | source)
XLA Modules:
  0.0 91.9 jit_solution(14223555700688407675)
XLA Ops:
  0.6 0.0 copy-start
  0.6 0.0 copy-start.7
  0.7 1.0 %fusion.50 = f32[8]{0:T(128)S(1)} fusion(bf16[8,2048]{1,0:T(8,128)(2,1)} %param.21), kind=kLoop, calls=%fused_computation.61 | loop fusion | flops 49144 | bytes 32800 | tf_op jit(solution)/shard_map/reduce_sum | solution.py:13
  1.7 1.4 %fusion.52 = bf16[8,2048]{1,0:T(8,128)(2,1)} fusion(bf16[8,2048]{1,0:T(8,128)(2,1)} %param.21, f32[2048]{0:T(1024)} %param.22, f32[8]{0:T(128)S(1)} %add_rsqrt_fusion.3), kind=kLoop, calls=%fused_computation.63 | loop fusion | flops 65536 | bytes 73760 | tf_op jit(solution)/shard_map/convert_element_type | solution.py:56
  3.2 6.4 %all-to-all-start = ((bf16[8,8,256]{2,0,1:T(8,128)(2,1)}), bf16[8,8,256]{2,0,1:T(8,128)(2,1)S(1)}, u32[]{:S(2)}, u32[]{:S(2)}) async-start(bf16[8,8,256]{2,0,1:T(8,128)(2,1)} %bitcast), calls=%async_computation | async-start | bytes 65536 | tf_op jit(solution)/shard_map/all_to_all | solution.py:57
  9.5 0.7 iota_compare_fusion.1
  10.2 0.8 copy.31
  11.0 0.1 eq.51
  11.1 0.2 convert_reduce_fusion.2
  11.3 0.1 reduce_sum.136
  11.3 0.1 copy.33
  11.4 0.1 fusion.82
  11.5 3.7 %all-to-all-done = bf16[8,8,256]{2,0,1:T(8,128)(2,1)S(1)} async-done(((bf16[8,8,256]{2,0,1:T(8,128)(2,1)}), bf16[8,8,256]{2,0,1:T(8,128)(2,1)S(1)}, u32[]{:S(2)}, u32[]{:S(2)}) %all-to-all-start) | async-done | bytes 32800 | tf_op jit(solution)/shard_map/all_to_all | solution.py:57
  15.2 1.9 %fusion.9 = bf16[8,8,1024]{2,1,0:T(8,128)(2,1)} fusion(bf16[256,1024]{1,0:T(8,128)(2,1)} %param.23, bf16[8,8,256]{2,0,1:T(8,128)(2,1)S(1)} %all-to-all-done), kind=kOutput, calls=%fused_computation.13 | convolution fusion | flops 33619968 | bytes 688128 | tf_op jit(solution)/shard_map/dot_general | solution.py:59
  17.2 3.4 %all-to-all-start.1 = ((bf16[8,8,1024]{2,1,0:T(8,128)(2,1)}), bf16[8,8,1024]{2,1,0:T(8,128)(2,1)S(1)}, u32[]{:S(2)}, u32[]{:S(2)}) async-start(bf16[8,8,1024]{2,1,0:T(8,128)(2,1)} %fusion.9), calls=%async_computation.1 | async-start | bytes 262144 | tf_op jit(solution)/shard_map/all_to_all | solution.py:20
  20.5 1.3 %convolution_convert_fusion.3 = bf16[8,8,1024]{2,1,0:T(8,128)(2,1)S(1)} fusion(bf16[256,1024]{1,0:T(8,128)(2,1)} %param.25, bf16[8,8,256]{2,0,1:T(8,128)(2,1)S(1)} %all-to-all-done), kind=kOutput, calls=%fused_computation.10 | convolution fusion | flops 33619968 | bytes 688128 | tf_op jit(solution)/shard_map/dot_general | solution.py:67
  21.8 1.3 %convolution_convert_fusion.4 = bf16[8,8,1024]{2,1,0:T(8,128)(2,1)S(1)} fusion(bf16[256,1024]{1,0:T(8,128)(2,1)} %param.24, bf16[8,8,256]{2,0,1:T(8,128)(2,1)S(1)} %all-to-all-done), kind=kOutput, calls=%fused_computation.11 | convolution fusion | flops 33619968 | bytes 688128 | tf_op jit(solution)/shard_map/dot_general | solution.py:66
  23.1 0.7 pad_maximum_fusion
  23.8 3.5 %all-to-all-done.1 = bf16[8,8,1024]{2,1,0:T(8,128)(2,1)S(1)} async-done(((bf16[8,8,1024]{2,1,0:T(8,128)(2,1)}), bf16[8,8,1024]{2,1,0:T(8,128)(2,1)S(1)}, u32[]{:S(2)}, u32[]{:S(2)}) %all-to-all-start.1) | async-done | bytes 131104 | tf_op jit(solution)/shard_map/all_to_all | solution.py:20
  27.2 0.1 fusion.62
  27.3 0.0 copy-done.7
  27.3 0.1 fusion.70
  27.4 0.0 copy-start.9
  27.4 5.8 %fusion.68 = f32[8,8,1,512]{3,2,1,0:T(1,128)S(1)} fusion(bf16[8,8,512,128]{3,2,1,0:T(8,128)(2,1)} %param.28, bf16[8,8,128,1]{2,0,1,3:T(8,128)(2,1)S(1)} %fusion.70), kind=kOutput, calls=%fused_computation.85 | convolution fusion | flops 8388608 | bytes 8536064 | tf_op jit(solution)/shard_map/shd,shld->shl/dot_general | solution.py:78
  33.2 0.0 copy-done.9
  33.2 0.6 fusion.16
  33.8 0.0 copy-done.1
  33.8 0.0 copy-start.2
  33.8 1.2 %fusion.33 = f32[8,8,1,128]{3,2,1,0:T(1,128)S(1)} fusion(bf16[8,8,512,128]{3,2,1,0:T(8,128)(2,1)S(1)} %copy-done.1, bf16[8,8,512,1]{2,1,0,3:T(8,128)(2,1)S(1)} %fusion.16), kind=kOutput, calls=%fused_computation.39 | convolution fusion | flops 8388608 | bytes 8486912 | tf_op jit(solution)/shard_map/shl,shld->shd/dot_general | solution.py:90
  35.0 0.0 copy-start.3
  35.0 1.0 %copy-done.2 = bf16[1024,2048]{1,0:T(8,128)(2,1)S(1)} copy-done((bf16[1024,2048]{1,0:T(8,128)(2,1)S(1)}, bf16[1024,2048]{1,0:T(8,128)(2,1)}, u32[]{:S(2)}) %copy-start.2) | copy-done | bytes 4194328
  36.0 0.7 convolution_convert_fusion.2
  36.7 8.6 %all-gather = bf16[32,2048]{1,0:T(8,128)(2,1)S(1)} all-gather(bf16[8,2048]{1,0:T(8,128)(2,1)S(1)} %convolution_convert_fusion.2), channel_id=2, replica_groups=mesh['ep'=8,'tp'=4] {'tp'}, dimensions={0}, use_global_device_ids=true | all-gather | bytes 163840 | tf_op jit(solution)/shard_map/all_gather | solution.py:93
  45.3 0.0 copy-done.4
  45.3 0.1 fusion.47
  45.4 0.0 copy-done.5
  45.4 0.2 convolution_convert_fusion
  45.7 0.0 copy-done.3
  45.7 0.3 fusion.91
  46.0 2.9 %convolution_convert_fusion.1 = bf16[8,2048]{1,0:T(8,128)(2,1)} fusion(bf16[256,2048]{1,0:T(8,128)(2,1)} %param.40, bf16[2048,256]{1,0:T(8,128)(2,1)} %param.39, f32[8,256]{1,0:T(8,128)S(1)} %fusion.91, bf16[8,2048]{1,0:T(8,128)(2,1)S(1)} %get-tuple-element.4, f32[2048]{0:T(1024)S(1)} %copy-done.5, f32[8]{0:T(128)S(1)} %add_rsqrt_fusion.2), kind=kOutput, calls=%fused_computation.8 | convolution fusion | flops 16871424 | bytes 2179104 | tf_op jit(solution)/shard_map/dot_general | solution.py:117
  48.9 3.3 %all-to-all-start.4 = ((bf16[4,8,512]{2,1,0:T(8,128)(2,1)}), bf16[4,8,512]{2,1,0:T(8,128)(2,1)S(1)}, u32[]{:S(2)}, u32[]{:S(2)}) async-start(bf16[4,8,512]{2,1,0:T(8,128)(2,1)} %bitcast.21), calls=%async_computation.4 | async-start | bytes 65536 | tf_op jit(solution)/shard_map/all_to_all | solution.py:123
  52.2 0.0 copy-done.6
  52.2 0.2 multiply_reduce_fusion
  52.4 0.7 all_to_all.44
  53.1 3.8 %all-to-all-done.4 = bf16[4,8,512]{2,1,0:T(8,128)(2,1)S(1)} async-done(((bf16[4,8,512]{2,1,0:T(8,128)(2,1)}), bf16[4,8,512]{2,1,0:T(8,128)(2,1)S(1)}, u32[]{:S(2)}, u32[]{:S(2)}) %all-to-all-start.4) | async-done | bytes 32800 | tf_op jit(solution)/shard_map/all_to_all | solution.py:123
  56.9 3.4 %all-to-all-start.2 = ((bf16[8,4,2048]{2,1,0:T(4,128)(2,1)}), bf16[8,4,2048]{2,1,0:T(4,128)(2,1)S(1)}, u32[]{:S(2)}, u32[]{:S(2)}) async-start(bf16[8,4,2048]{2,1,0:T(4,128)(2,1)} %all_to_all.44), calls=%async_computation.2 | async-start | bytes 262144 | tf_op jit(solution)/shard_map/all_to_all | solution.py:112
  60.3 6.7 %all-to-all-done.2 = bf16[8,4,2048]{2,1,0:T(4,128)(2,1)S(1)} async-done(((bf16[8,4,2048]{2,1,0:T(4,128)(2,1)}), bf16[8,4,2048]{2,1,0:T(4,128)(2,1)S(1)}, u32[]{:S(2)}, u32[]{:S(2)}) %all-to-all-start.2) | async-done | bytes 131104 | tf_op jit(solution)/shard_map/all_to_all | solution.py:112
  66.9 3.4 %all-to-all-start.5 = ((bf16[8,8,2048]{2,1,0:T(8,128)(2,1)}), bf16[8,8,2048]{2,1,0:T(8,128)(2,1)S(1)}, u32[]{:S(2)}, u32[]{:S(2)}) async-start(bf16[8,8,2048]{2,1,0:T(8,128)(2,1)} %pad_maximum_fusion), calls=%async_computation.5 | async-start | bytes 524288 | tf_op jit(solution)/shard_map/all_to_all | solution.py:20
  70.4 2.3 %fusion.4 = f32[32,640]{1,0:T(8,128)S(1)} fusion(bf16[32,2048]{1,0:T(8,128)(2,1)S(1)} %all_to_all.46, bf16[1,2048,640]{2,1,0:T(8,128)(2,1)} %param.35), kind=kOutput, calls=%fused_computation.4 | convolution fusion | flops 83886080 | bytes 2834432 | tf_op jit(solution)/shard_map/dot_general | solution.py:132
  72.7 0.0 copy-done
  72.7 0.0 copy-start.8
  72.7 2.7 %fusion.6 = bf16[32,2048]{1,0:T(8,128)(2,1)S(1)} fusion(bf16[1,640,2048]{2,1,0:T(8,128)(2,1)S(1)} %copy-done, bf16[32,2048]{1,0:T(8,128)(2,1)S(1)} %all_to_all.46, bf16[1,2048,640]{2,1,0:T(8,128)(2,1)} %param.36, f32[32,640]{1,0:T(8,128)S(1)} %fusion.4), kind=kOutput, calls=%fused_computation.6 | convolution fusion | flops 167960576 | bytes 5586944 | tf_op jit(solution)/shard_map/dot_general | solution.py:135
  75.4 0.1 reshape.169
  75.5 0.7 copy.35
  76.2 3.8 %all-to-all-done.5 = bf16[8,8,2048]{2,1,0:T(8,128)(2,1)S(1)} async-done(((bf16[8,8,2048]{2,1,0:T(8,128)(2,1)}), bf16[8,8,2048]{2,1,0:T(8,128)(2,1)S(1)}, u32[]{:S(2)}, u32[]{:S(2)}) %all-to-all-start.5) | async-done | bytes 262176 | tf_op jit(solution)/shard_map/all_to_all | solution.py:20
  80.0 2.6 %all-to-all-start.3 = ((bf16[32,4,512]{2,1,0:T(4,128)(2,1)}), bf16[32,4,512]{2,1,0:T(4,128)(2,1)S(1)}, u32[]{:S(2)}, u32[]{:S(2)}) async-start(bf16[32,4,512]{2,1,0:T(4,128)(2,1)} %bitcast.18), calls=%async_computation.3 | async-start | bytes 262144 | tf_op jit(solution)/shard_map/all_to_all | solution.py:137
  82.6 0.1 fusion.60
  82.7 0.6 slice.9
  83.3 0.7 fusion.61
  84.0 6.9 %all-to-all-done.3 = bf16[32,4,512]{2,1,0:T(4,128)(2,1)S(1)} async-done(((bf16[32,4,512]{2,1,0:T(4,128)(2,1)}), bf16[32,4,512]{2,1,0:T(4,128)(2,1)S(1)}, u32[]{:S(2)}, u32[]{:S(2)}) %all-to-all-start.3) | async-done | bytes 131104 | tf_op jit(solution)/shard_map/all_to_all | solution.py:137
  91.0 0.1 bitcast_reduce_fusion
  91.0 0.0 copy-done.8
  91.0 0.2 fusion.20
  91.2 0.7 add_convert_fusion
  (17 shorter events, 0.2 us)
Async XLA Ops:
  0.6 72.0 %copy-start = (bf16[1,640,2048]{2,1,0:T(8,128)(2,1)S(1)}, bf16[1,640,2048]{2,1,0:T(8,128)(2,1)}, u32[]{:S(2)}) copy-start(bf16[1,640,2048]{2,1,0:T(8,128)(2,1)} %param.37) | copy-start | bytes 7864324
  0.6 26.7 %copy-start.7 = (f32[128]{0:T(128)S(1)}, f32[128]{0:T(128)}, u32[]{:S(2)}) copy-start(f32[128]{0:T(128)} %param.26) | copy-start | bytes 1540
  3.2 12.1 %all-to-all-start = ((bf16[8,8,256]{2,0,1:T(8,128)(2,1)}), bf16[8,8,256]{2,0,1:T(8,128)(2,1)S(1)}, u32[]{:S(2)}, u32[]{:S(2)}) async-start(bf16[8,8,256]{2,0,1:T(8,128)(2,1)} %bitcast), calls=%async_computation | async-start | bytes 65536 | tf_op jit(solution)/shard_map/all_to_all | solution.py:57
  17.2 10.1 %all-to-all-start.1 = ((bf16[8,8,1024]{2,1,0:T(8,128)(2,1)}), bf16[8,8,1024]{2,1,0:T(8,128)(2,1)S(1)}, u32[]{:S(2)}, u32[]{:S(2)}) async-start(bf16[8,8,1024]{2,1,0:T(8,128)(2,1)} %fusion.9), calls=%async_computation.1 | async-start | bytes 262144 | tf_op jit(solution)/shard_map/all_to_all | solution.py:20
  27.4 5.8 %copy-start.9 = (f32[8]{0:T(128)S(1)}, f32[8]{0:T(128)}, u32[]{:S(2)}) copy-start(f32[8]{0:T(128)} %param.27) | copy-start | bytes 100
  27.4 6.4 %copy-start.1 = (bf16[8,8,512,128]{3,2,1,0:T(8,128)(2,1)S(1)}, bf16[8,8,512,128]{3,2,1,0:T(8,128)(2,1)}, u32[]{:S(2)}) copy-start(bf16[8,8,512,128]{3,2,1,0:T(8,128)(2,1)} %param.29) | copy-start | bytes 25165828
  33.8 2.2 %copy-start.2 = (bf16[1024,2048]{1,0:T(8,128)(2,1)S(1)}, bf16[1024,2048]{1,0:T(8,128)(2,1)}, u32[]{:S(2)}) copy-start(bf16[1024,2048]{1,0:T(8,128)(2,1)} %param.31) | copy-start | bytes 12582916
  35.0 10.3 %copy-start.4 = (bf16[8,2048]{1,0:T(8,128)(2,1)S(1)}, bf16[8,2048]{1,0:T(8,128)(2,1)}, u32[]{:S(2)}) copy-start(bf16[8,2048]{1,0:T(8,128)(2,1)} %param.21) | copy-start | bytes 98308
  35.0 10.4 %copy-start.5 = (f32[2048]{0:T(1024)S(1)}, f32[2048]{0:T(1024)}, u32[]{:S(2)}) copy-start(f32[2048]{0:T(1024)} %param.32) | copy-start | bytes 24580
  35.0 10.7 %copy-start.3 = (bf16[2048,256]{1,0:T(8,128)(2,1)S(1)}, bf16[2048,256]{1,0:T(8,128)(2,1)}, u32[]{:S(2)}) copy-start(bf16[2048,256]{1,0:T(8,128)(2,1)} %param.38) | copy-start | bytes 3145732
  36.7 15.5 %copy-start.6 = (f32[2048]{0:T(1024)S(1)}, f32[2048]{0:T(1024)}, u32[]{:S(2)}) copy-start(f32[2048]{0:T(1024)} %param.41) | copy-start | bytes 24580
  48.9 8.0 %all-to-all-start.4 = ((bf16[4,8,512]{2,1,0:T(8,128)(2,1)}), bf16[4,8,512]{2,1,0:T(8,128)(2,1)S(1)}, u32[]{:S(2)}, u32[]{:S(2)}) async-start(bf16[4,8,512]{2,1,0:T(8,128)(2,1)} %bitcast.21), calls=%async_computation.4 | async-start | bytes 65536 | tf_op jit(solution)/shard_map/all_to_all | solution.py:123
  56.9 10.1 %all-to-all-start.2 = ((bf16[8,4,2048]{2,1,0:T(4,128)(2,1)}), bf16[8,4,2048]{2,1,0:T(4,128)(2,1)S(1)}, u32[]{:S(2)}, u32[]{:S(2)}) async-start(bf16[8,4,2048]{2,1,0:T(4,128)(2,1)} %all_to_all.44), calls=%async_computation.2 | async-start | bytes 262144 | tf_op jit(solution)/shard_map/all_to_all | solution.py:112
  66.9 13.1 %all-to-all-start.5 = ((bf16[8,8,2048]{2,1,0:T(8,128)(2,1)}), bf16[8,8,2048]{2,1,0:T(8,128)(2,1)S(1)}, u32[]{:S(2)}, u32[]{:S(2)}) async-start(bf16[8,8,2048]{2,1,0:T(8,128)(2,1)} %pad_maximum_fusion), calls=%async_computation.5 | async-start | bytes 524288 | tf_op jit(solution)/shard_map/all_to_all | solution.py:20
  72.7 18.4 %copy-start.8 = (f32[8,2]{0,1:T(2,128)S(1)}, f32[8,2]{0,1:T(2,128)}, u32[]{:S(2)}) copy-start(f32[8,2]{0,1:T(2,128)} %param.34) | copy-start | bytes 196
  80.0 10.9 %all-to-all-start.3 = ((bf16[32,4,512]{2,1,0:T(4,128)(2,1)}), bf16[32,4,512]{2,1,0:T(4,128)(2,1)S(1)}, u32[]{:S(2)}, u32[]{:S(2)}) async-start(bf16[32,4,512]{2,1,0:T(4,128)(2,1)} %bitcast.18), calls=%async_computation.3 | async-start | bytes 262144 | tf_op jit(solution)/shard_map/all_to_all | solution.py:137

commit v2 on v1

--- a/solution.py
+++ b/solution.py
@@ -1,9 +1,14 @@
 import jax
 import jax.numpy as jnp
 from jax import lax
+from jax.experimental import pallas as pl
+from jax.experimental.pallas import tpu as pltpu
 from jax.sharding import PartitionSpec as P
 
+
 DH = 128
+COPY_BYTES = 1 << 20
+LANES = 128
 
 
 epsilon = 1e-06
@@ -23,7 +28,7 @@
     return jnp.sum(blocks.reshape(count, rows, -1).astype(jnp.float32), axis=0)
 
 
-def body(
+def plain_layer(
     tokens,
     attn_gain,
     query_weight,
@@ -155,6 +160,427 @@
     return (mixed, new_keys, new_values)
 
 
+def in_vmem(count):
+    return [pl.BlockSpec(memory_space=pltpu.VMEM)] * count
+
+
+def call(kernel, outs, *arrays, scalars=0, limit=8 << 20):
+    return pl.pallas_call(
+        kernel,
+        out_shape=[jax.ShapeDtypeStruct(shape, dtype) for shape, dtype in outs],
+        in_specs=[pl.BlockSpec(memory_space=pltpu.SMEM)] * scalars
+        + in_vmem(len(arrays) - scalars),
+        out_specs=in_vmem(len(outs)),
+        compiler_params=pltpu.CompilerParams(vmem_limit_bytes=limit),
+    )(*arrays)
+
+
+def stage(*groups):
+    plan, shapes = [], []
+    for target, group in enumerate(groups):
+        offset = 0
+        for array in group:
+            size = array.size * array.dtype.itemsize
+            count = max(1, size // COPY_BYTES)
+            while array.shape[0] % count:
+                count -= 1
+            plan.append((target, offset, array.shape[0] // count, count))
+            offset += array.shape[0]
+        shapes.append(pltpu.VMEM((offset,) + group[0].shape[1:], group[0].dtype))
+    arrays = [array for group in groups for array in group]
+    total = sum(count for *_, count in plan)
+
+    def kernel(*refs):
+        sources, targets, sems = refs[: len(arrays)], refs[len(arrays) : -1], refs[-1]
+        copies = []
+        for source, (target, offset, rows, count) in zip(sources, plan):
+            for i in range(count):
+                copies.append(
+                    pltpu.make_async_copy(
+                        source.at[pl.ds(i * rows, rows)],
+                        targets[target].at[pl.ds(offset + i * rows, rows)],
+                        sems.at[len(copies)],
+                    )
+                )
+        for copy in copies:
+            copy.start()
+        for copy in copies:
+            copy.wait()
+
+    return pl.pallas_call(
+        kernel,
+        out_shape=shapes,
+        in_specs=[pl.BlockSpec(memory_space=pltpu.HBM) for _ in arrays],
+        out_specs=in_vmem(len(groups)),
+        scratch_shapes=[pltpu.SemaphoreType.DMA((total,))],
+        compiler_params=pltpu.CompilerParams(vmem_limit_bytes=1 << 20),
+    )(*[pltpu.with_memory_space_constraint(array, pltpu.HBM) for array in arrays])
+
+
+def place():
+    index = lax.axis_index("ep")
+    return lax.div(index, jnp.int32(2)), lax.rem(index, jnp.int32(2))
+
+
+def pair_move(values):
+    count = lax.axis_size("ep")
+    return lax.ppermute(values, "ep", [(i, i ^ 1) for i in range(count)])
+
+
+def far_move(values, step):
+    count = lax.axis_size("ep")
+    return lax.ppermute(values, "ep", [(i, i ^ (2 * step)) for i in range(count)])
+
+
+def tp_move(values, turn):
+    count = lax.axis_size("tp")
+    return lax.ppermute(values, "tp", [(i, i ^ turn) for i in range(count)])
+
+
+def aligned(index, size):
+    return pl.multiple_of(index * size, size)
+
+
+def split_tokens(tokens):
+    rows, width = tokens.shape
+    count = lax.axis_size("ep")
+    features = width // count
+    half = count // 2
+
+    def kernel(tokens_ref, away_ref, kept_ref, scale_ref):
+        high, low = place()
+        for step in range(half):
+            for target, side in ((kept_ref, low), (away_ref, 1 - low)):
+                column = aligned(2 * (high ^ step) + side, features)
+                target[step] = tokens_ref[:, pl.ds(column, features)]
+        stream = tokens_ref[...].astype(jnp.float32)
+        mean_square = jnp.mean(stream * stream, axis=-1, keepdims=True)
+        scale_ref[...] = jnp.broadcast_to(lax.rsqrt(mean_square + epsilon), scale_ref.shape)
+
+    shape = (half, rows, features)
+    return call(
+        kernel,
+        [(shape, tokens.dtype), (shape, tokens.dtype), ((rows, LANES), jnp.float32)],
+        tokens,
+    )
+
+
+def knit(kept, came):
+    half, rows, width = kept.shape
+
+    def kernel(kept_ref, came_ref, *outs):
+        for step, out_ref in enumerate(outs):
+            out_ref[...] = jnp.concatenate([kept_ref[step], came_ref[step]], axis=0)
+
+    return call(kernel, [((2 * rows, width), kept.dtype)] * half, kept, came)
+
+
+def project(parts, gain, weights, parts_out):
+    features = parts[0].shape[1]
+    rows = parts[0].shape[0] // 2
+    half = len(parts)
+    wide = weights.shape[1]
+
+    def kernel(*refs):
+        part_refs, (gain_ref, weight_ref, away_ref, kept_ref) = refs[:half], refs[half:]
+        gain_part = gain_ref[:, pl.ds(aligned(lax.axis_index("ep"), features), features)]
+        values = [ref[...].astype(jnp.float32) for ref in part_refs]
+        ordered = [value[rows:] for value in values] + [value[:rows] for value in values]
+        lines = (jnp.concatenate(ordered, axis=0) * gain_part).astype(jnp.bfloat16)
+        for i in range(parts_out):
+            weight = weight_ref[i * features : (i + 1) * features, :]
+            part = jnp.dot(lines, weight, preferred_element_type=jnp.float32)
+            away_ref[:, i * wide : (i + 1) * wide] = part[: half * rows].astype(jnp.bfloat16)
+            kept_ref[:, i * wide : (i + 1) * wide] = part[half * rows :]
+
+    shape = (half * rows, parts_out * wide)
+    return call(
+        kernel,
+        [(shape, jnp.bfloat16), (shape, jnp.float32)],
+        *parts,
+        gain.reshape(1, -1),
+        weights,
+        limit=16 << 20,
+    )
+
+
+def slots_of(ids_ref):
+    chosen = []
+    for b in range(ids_ref.shape[1]):
+        for k in range(ids_ref.shape[0]):
+            expert = ids_ref[k, b]
+            slot = jnp.int32(0)
+            for _, _, other, _ in chosen:
+                slot = slot + (other == expert).astype(jnp.int32)
+            chosen.append((b, k, expert, slot))
+    return chosen
+
+
+def dispatch(ids, weights, tokens, attn_parts, mix_gain, capacity):
+    rows, width = tokens.shape
+    count, tp_size = lax.axis_size("ep"), lax.axis_size("tp")
+    half = count // 2
+    col_width = width // tp_size
+    slots = half * capacity
+    terms = len(attn_parts)
+
+    def kernel(ids_ref, weights_ref, tokens_ref, *refs):
+        part_refs, gain_ref = refs[:terms], refs[terms]
+        middle_ref, kept_ref, away_ref, scratch = refs[terms + 1 :]
+        proj = part_refs[0][...].astype(jnp.float32)
+        for ref in part_refs[1:]:
+            proj = proj + ref[...].astype(jnp.float32)
+        middle = (tokens_ref[...].astype(jnp.float32) + proj).astype(jnp.bfloat16)
+        wide = middle.astype(jnp.float32)
+        scratch[...] = wide
+        column = aligned(lax.axis_index("tp"), col_width)
+        middle_ref[...] = scratch[:, pl.ds(column, col_width)]
+        mean_square = jnp.mean(wide * wide, axis=-1, keepdims=True)
+        normed = (wide * lax.rsqrt(mean_square + epsilon) * gain_ref[...]).astype(jnp.bfloat16)
+        high, low = place()
+        line = lax.broadcasted_iota(jnp.int32, (2 * slots, LANES), 0)
+        lane = lax.broadcasted_iota(jnp.int32, (2 * slots, LANES), 1)
+        picks = jnp.zeros((2 * slots, LANES), jnp.float32)
+        share = jnp.zeros((2 * slots, LANES), jnp.float32)
+        first = jnp.zeros((2 * slots, LANES), jnp.float32)
+        for b, k, expert, slot in slots_of(ids_ref):
+            block = lax.div(expert, jnp.int32(2)) ^ high
+            side = lax.rem(expert, jnp.int32(2)) ^ low
+            here = line == side * slots + block * capacity + slot
+            picks = jnp.where(here & (lane == b), 1.0, picks)
+            share = jnp.where(here, weights_ref[k, b], share)
+            if k == 0:
+                first = jnp.where(here, 1.0, first)
+        outbox = jnp.dot(
+            picks[:, :rows].astype(jnp.bfloat16), normed, preferred_element_type=jnp.float32
+        ).astype(jnp.bfloat16)
+        upper = share.astype(jnp.bfloat16).astype(jnp.float32)
+        notes = jnp.where(lane == 0, upper, jnp.where(lane == 1, share - upper, first))
+        notes = notes.astype(jnp.bfloat16)
+        kept_ref[:, :width] = outbox[:slots]
+        away_ref[:, :width] = outbox[slots:]
+        kept_ref[:, width:] = notes[:slots]
+        away_ref[:, width:] = notes[slots:]
+
+    shape = (slots, width + LANES)
+    return pl.pallas_call(
+        kernel,
+        out_shape=[
+            jax.ShapeDtypeStruct((rows, col_width), jnp.float32),
+            jax.ShapeDtypeStruct(shape, jnp.bfloat16),
+            jax.ShapeDtypeStruct(shape, jnp.bfloat16),
+        ],
+        in_specs=[pl.BlockSpec(memory_space=pltpu.SMEM)] * 2 + in_vmem(terms + 2),
+        out_specs=in_vmem(3),
+        scratch_shapes=[pltpu.VMEM((rows, width), jnp.float32)],
+        compiler_params=pltpu.CompilerParams(vmem_limit_bytes=8 << 20),
+    )(ids, weights, tokens, *attn_parts, mix_gain.reshape(1, -1))
+
+
+def experts_apply(parts, gate_up, down, side_in, side_back, branch_gate, capacity):
+    count, tp_size = lax.axis_size("ep"), lax.axis_size("tp")
+    width = parts[0].shape[1] - LANES
+    col_width = width // tp_size
+    chunks = col_width // LANES
+
+    def kernel(*refs):
+        part_refs = refs[: len(parts)]
+        gate_up_ref, down_ref, side_in_ref, side_back_ref, branch_ref, out_ref = refs[len(parts) :]
+        whole = jnp.concatenate([ref[...] for ref in part_refs], axis=0)
+        lines = whole[:, :width]
+        notes = whole[:, width:].astype(jnp.float32)
+        share = notes[:, 0:1] + notes[:, 1:2]
+        logit = jnp.sum(lines.astype(jnp.float32) * branch_ref[...], axis=1, keepdims=True)
+        switch = notes[:, 2:3] * jax.nn.sigmoid(logit)
+
+        def hidden_of(ref):
+            gate_pre = jnp.dot(lines, ref[:width, :], preferred_element_type=jnp.float32)
+            up_pre = jnp.dot(lines, ref[width:, :], preferred_element_type=jnp.float32)
+            return (jax.nn.silu(gate_pre) * up_pre).astype(jnp.bfloat16)
+
+        hidden = hidden_of(gate_up_ref)
+        side_hidden = hidden_of(side_in_ref)
+        high, low = place()
+        for t in range(tp_size):
+            columns = slice(t * col_width, (t + 1) * col_width)
+            result = share * jnp.dot(
+                hidden, down_ref[:, columns], preferred_element_type=jnp.float32
+            ) + switch * jnp.dot(
+                side_hidden, side_back_ref[:, columns], preferred_element_type=jnp.float32
+            )
+            for step in range(count // 2):
+                for part in range(2):
+                    source = 2 * (high ^ step) + (low ^ part)
+                    start = (2 * step + part) * capacity
+                    block = jnp.concatenate(
+                        [
+                            result[start : start + capacity, c * LANES : (c + 1) * LANES]
+                            for c in range(chunks)
+                        ],
+                        axis=0,
+                    )
+                    out_ref[source * tp_size + t] = block.astype(jnp.bfloat16)
+
+    shape = (count * tp_size, chunks * capacity, LANES)
+    return call(
+        kernel,
+        [(shape, jnp.bfloat16)],
+        *parts,
+        gate_up,
+        down,
+        side_in,
+        side_back,
+        branch_gate.reshape(1, -1),
+        limit=12 << 20,
+    )[0]
+
+
+def home_picks(ids, rows, capacity, chunks):
+    count, tp_size = lax.axis_size("ep"), lax.axis_size("tp")
+    per_block = chunks * capacity
+    total = count * tp_size * per_block
+
+    def kernel(ids_ref, out_ref):
+        row = lax.broadcasted_iota(jnp.int32, (chunks * rows, total), 0)
+        column = lax.broadcasted_iota(jnp.int32, (chunks * rows, total), 1)
+        expert_of = lax.div(column, jnp.int32(tp_size * per_block))
+        within = lax.rem(column, jnp.int32(per_block))
+        same = lax.div(within, jnp.int32(capacity)) == lax.div(row, jnp.int32(rows))
+        key = expert_of * capacity + lax.rem(within, jnp.int32(capacity))
+        token = lax.rem(row, jnp.int32(rows))
+        picks = jnp.zeros((chunks * rows, total), jnp.float32)
+        for b, _, expert, slot in slots_of(ids_ref):
+            hit = (key == expert * capacity + slot) & (token == b)
+            picks = jnp.where(hit, 1.0, picks)
+        out_ref[...] = jnp.where(same, picks, 0.0).astype(jnp.bfloat16)
+
+    shape = (chunks * rows, total)
+    return call(kernel, [(shape, jnp.bfloat16)], ids, scalars=1)[0]
+
+
+def finish(picks, returned, middle):
+    rows, col_width = middle.shape
+    chunks = col_width // LANES
+
+    def kernel(picks_ref, returned_ref, middle_ref, out_ref):
+        lines = returned_ref[...].reshape(-1, LANES)
+        sums = jnp.dot(picks_ref[...], lines, preferred_element_type=jnp.float32)
+        for c in range(chunks):
+            columns = slice(c * LANES, (c + 1) * LANES)
+            total = middle_ref[:, columns] + sums[c * rows : (c + 1) * rows]
+            out_ref[:, columns] = total.astype(jnp.bfloat16)
+
+    return call(kernel, [((rows, col_width), jnp.bfloat16)], picks, returned, middle)[0]
+
+
+def fast_layer(
+    tokens,
+    attn_gain,
+    query_weight,
+    key_weight,
+    value_weight,
+    query_gain,
+    stick_bias,
+    key_cache,
+    value_cache,
+    lengths,
+    out_weight,
+    mix_gain,
+    route_ids,
+    route_weights,
+    expert_gate,
+    expert_up,
+    expert_down,
+    side_gate,
+    side_up,
+    side_down,
+    branch_gate,
+):
+    seq_count, model_width = tokens.shape
+    head_cols = query_weight.shape[1]
+    heads_local = key_cache.shape[1]
+    cache_slots = key_cache.shape[2]
+    experts, tp_size = lax.axis_size("ep"), lax.axis_size("tp")
+    half = experts // 2
+    top_count = route_ids.shape[1]
+    capacity = max(2, 2 * top_count * seq_count // experts)
+
+    away, kept, scales = split_tokens(tokens)
+    came = pair_move(away)
+    parts = knit(kept, came)
+    parts = [parts[0]] + [far_move(parts[step], step) for step in range(1, half)]
+    key_cache, weights = stage([key_cache], [query_weight, key_weight, value_weight])
+    away, kept = project(parts, attn_gain, weights, 3)
+    came = pair_move(away)
+    both = kept + came.astype(jnp.float32)
+    projected = both[:seq_count]
+    for step in range(1, half):
+        leaving = both[step * seq_count : (step + 1) * seq_count].astype(jnp.bfloat16)
+        moved = far_move(leaving, step)
+        projected = projected + moved.astype(jnp.float32)
+    projected = (projected * scales[:, :1]).astype(jnp.bfloat16)
+    query_rows = projected[:, :head_cols]
+    fresh_keys = projected[:, head_cols : 2 * head_cols].astype(jnp.float32)
+    new_values = projected[:, 2 * head_cols :]
+    new_keys = rms_scale(fresh_keys.reshape(seq_count, heads_local, DH), 1.0)
+    new_keys = new_keys.astype(jnp.bfloat16).reshape(seq_count, head_cols)
+    query_heads = rms_scale(
+        query_rows.astype(jnp.float32).reshape(seq_count, heads_local, DH), query_gain
+    ).astype(jnp.bfloat16)
+    value_cache, out_weight = stage([value_cache], [out_weight])
+
+    scores = jnp.einsum("shd,shld->shl", query_heads, key_cache, preferred_element_type=jnp.float32)
+    scores = scores * DH ** (-0.5) + stick_bias[None, :, None]
+    positions = jnp.arange(cache_slots, dtype=jnp.int32)
+    visible = positions[None, None, :] < lengths[:, None, None]
+    log_rest = jnp.where(visible, jax.nn.log_sigmoid(-scores), 0.0)
+    later = (positions[:, None] > positions[None, :]).astype(jnp.float32)
+    log_between = jnp.dot(
+        log_rest.reshape(-1, cache_slots), later, precision=lax.Precision.HIGHEST
+    ).reshape(scores.shape)
+    stick = jnp.where(visible, jnp.exp(jax.nn.log_sigmoid(scores) + log_between), 0.0).astype(
+        jnp.bfloat16
+    )
+    attended = jnp.einsum("shl,shld->shd", stick, value_cache, preferred_element_type=jnp.float32)
+    attended = attended.astype(jnp.bfloat16).reshape(seq_count, head_cols)
+    attn_part = jnp.dot(attended, out_weight, preferred_element_type=jnp.float32)
+    attn_part = attn_part.astype(jnp.bfloat16)
+    attn_parts = [attn_part] + [tp_move(attn_part, turn) for turn in range(1, tp_size)]
+    side_in, side_back = stage([side_gate, side_up], [side_down])
+
+    ids, weights_t = route_ids.T, route_weights.T
+    middle, kept, away = dispatch(ids, weights_t, tokens, attn_parts, mix_gain, capacity)
+    came = pair_move(away)
+    kept = kept.reshape(half, capacity, -1)
+    came = came.reshape(half, capacity, -1)
+    parts = [jnp.concatenate([kept[step], came[step]], axis=0) for step in range(half)]
+    parts = [parts[0]] + [far_move(parts[step], step) for step in range(1, half)]
+    (gate_up,) = stage([expert_gate[0], expert_up[0]])
+    blocks = experts_apply(
+        parts, gate_up, expert_down[0], side_in, side_back, branch_gate, capacity
+    )
+    returned = lax.all_to_all(
+        blocks, ("ep", "tp"), split_axis=0, concat_axis=0, tiled=True
+    )
+    picks = home_picks(ids, seq_count, capacity, model_width // tp_size // LANES)
+    mixed = finish(picks, returned, middle)
+    return (mixed, new_keys, new_values)
+
+
+def two_power(count):
+    return count & (count - 1) == 0
+
+
+def body(*arrays):
+    tokens = arrays[0]
+    experts, tp_size = lax.axis_size("ep"), lax.axis_size("tp")
+    widths = (tokens.shape[1] // experts, tokens.shape[1] // tp_size, arrays[14].shape[2])
+    fits = experts > 1 and two_power(experts) and two_power(tp_size)
+    fits = fits and all(width % LANES == 0 for width in widths)
+    fits = fits and tokens.shape[0] == 8
+    return (fast_layer if fits else plain_layer)(*arrays)
+
+
 def solution(mesh):
     in_specs = (
         P("ep", None),

time: 92.9 us -> 65.3 us (0.70)
  Pallas kernels: 0 us -> 18.8 us
  matrix products: 21.2 us -> 4.68 us
  waiting for transfers between devices: 28.4 us -> 14.7 us
  blocking collectives: 8.59 us -> 0 us
  other arithmetic: 6.32 us -> 1.16 us
  local copies, waits for them, and re-layouts: 4.18 us -> 1.6 us
    all_to_all x6 -> x1, waiting for transfers between devices: 28.4 us -> 7.08 us  [fast_layer(): lax.all_to_all(blocks, ('ep', 'tp'), split_axis=0, concat_axis=0, tiled=T...]
    pallas_call x0 -> x11, Pallas kernels: none -> 18.8 us  [the longest x4 13.2 us: stage(): pl.pallas_call(kernel, out_shape=shapes, in_specs=[pl.BlockSpec(memory_sp...]
    ppermute x0 -> x15, starting transfers between devices: none -> 18.7 us  [the longest x9 14.6 us: far_move(): return lax.ppermute(values, 'ep', [(i, i ^ 2 * step) for i in range(count)])]
    all_to_all x6 -> x1, starting transfers between devices: 22.3 us -> 4.44 us  [fast_layer(): lax.all_to_all(blocks, ('ep', 'tp'), split_axis=0, concat_axis=0, tiled=T...]
    dot_general x13 -> x4, matrix products: 21.2 us -> 4.68 us  [the longest x1 2.26 us: fast_layer(): jnp.einsum('shd,shld->shl', query_heads, key_cache, preferred_element_typ...]
    all_gather x1 -> x0, blocking collectives: 8.59 us -> none  [body(): lax.all_gather(attn_part.astype(jnp.bfloat16), 'tp', axis=0, tiled=False)]
    ppermute x0 -> x15, waiting for transfers between devices: none -> 7.58 us  [the longest x9 4.18 us: far_move(): return lax.ppermute(values, 'ep', [(i, i ^ 2 * step) for i in range(count)])]
    convert_element_type x4 -> x3, other arithmetic: 2.87 us -> 0.84 us  [the longest x1 0.68 us: fast_layer(): new_keys = new_keys.astype(jnp.bfloat16).reshape(seq_count, head_cols)]
  transfers between devices with their start and end apart: 6 -> 16, of which waited for: 6 -> 7; matrix products, arithmetic and copies ran while one was open for 14% -> 2% of each run, Pallas kernels for 0% -> 21%
where the time goes in v2:
time: 65.3 us; the launch traced here: 65.1 us
  starting transfers between devices  23.2 us (36%)
  Pallas kernels  18.8 us (29%)
  waiting for transfers between devices  14.7 us (23%)
  matrix products  4.68 us (7%)
  local copies, waits for them, and re-layouts  1.6 us (2%)
  other arithmetic  1.16 us (2%)
  between operations  0.99 us (2%)
    ppermute x9, starting transfers between devices, far_move(): return lax.ppermute(values, 'ep', [(i, i ^ 2 * step) for i in range(count)])  14.6 us
    pallas_call x4, Pallas kernels, stage(): pl.pallas_call(kernel, out_shape=shapes, in_specs=[pl.BlockSpec(memory_sp...  13.2 us
    all_to_all x1, waiting for transfers between devices, fast_layer(): lax.all_to_all(blocks, ('ep', 'tp'), split_axis=0, concat_axis=0, tiled=T...  7.08 us
    pallas_call x6, Pallas kernels, call(): pl.pallas_call(kernel, out_shape=[jax.ShapeDtypeStruct(shape, dtype) for...  4.66 us
    all_to_all x1, starting transfers between devices, fast_layer(): lax.all_to_all(blocks, ('ep', 'tp'), split_axis=0, concat_axis=0, tiled=T...  4.44 us
    ppermute x9, waiting for transfers between devices, far_move(): return lax.ppermute(values, 'ep', [(i, i ^ 2 * step) for i in range(count)])  4.18 us
    ppermute x3, starting transfers between devices, tp_move(): return lax.ppermute(values, 'tp', [(i, i ^ turn) for i in range(count)])  3.5 us
    ppermute x3, waiting for transfers between devices, pair_move(): return lax.ppermute(values, 'ep', [(i, i ^ 1) for i in range(count)])  3.39 us
  transfers between devices with their start and end apart: 16, of which 7 were waited for; matrix products, arithmetic and copies ran while one was open for 2% of the time, Pallas kernels for 21%

profile of v2, /device:TPU:0, one launch (start us, length us, event | category | flops | bytes accessed | tf_op | source)
XLA Modules:
  0.0 65.1 jit_solution(2518916860196126062)
XLA Ops:
  0.6 0.0 copy-start.1
  0.6 0.7 %copy-done.1 = bf16[8,2048]{1,0:T(8,128)(2,1)S(1)} copy-done((bf16[8,2048]{1,0:T(8,128)(2,1)S(1)}, bf16[8,2048]{1,0:T(8,128)(2,1)}, u32[]{:S(2)}) %copy-start.1) | copy-done | bytes 32792
  1.4 0.1 shard_map.221
  1.5 0.5 collective-permute-start
  2.0 0.8 %collective-permute-done.came_ref = bf16[4,8,256]{2,1,0:T(8,128)(2,1)S(1)} collective-permute-done((bf16[4,8,256]{2,1,0:T(8,128)(2,1)S(1)}, bf16[4,8,256]{2,1,0:T(8,128)(2,1)S(1)}, u32[]{:S(2)}, u32[]{:S(2)}) %collective-permute-start) | collective-permute-done | bytes 16416 | tf_op jit(solution)/shard_map/ppermute | solution.py:227
  2.8 3.0 %collective-permute-start.1 = (bf16[16,256]{1,0:T(8,128)(2,1)S(1)}, bf16[16,256]{1,0:T(8,128)(2,1)S(1)}, u32[]{:S(2)}, u32[]{:S(2)}) collective-permute-start(bf16[16,256]{1,0:T(8,128)(2,1)S(1)} %get-tuple-element.24), channel_id=1, source_target_pairs={{0,8},{4,12},{8,0},{12,4},{16,24},{20,28},{24,16},{28,20},{1,9},{5... | collective-permute-start | bytes 24584 | tf_op jit(solution)/shard_map/ppermute | solution.py:232
  5.8 2.6 %collective-permute-start.2 = (bf16[16,256]{1,0:T(8,128)(2,1)S(1)}, bf16[16,256]{1,0:T(8,128)(2,1)S(1)}, u32[]{:S(2)}, u32[]{:S(2)}) collective-permute-start(bf16[16,256]{1,0:T(8,128)(2,1)S(1)} %get-tuple-element.25), channel_id=1, source_target_pairs={{0,16},{4,20},{8,24},{12,28},{16,0},{20,4},{24,8},{28,12},{1,17},{... | collective-permute-start | bytes 24584 | tf_op jit(solution)/shard_map/ppermute | solution.py:232
  8.4 0.0 collective-permute-start.3
  8.4 3.9 %shard_map.223 = (bf16[8,8,512,128]{3,2,1,0:T(8,128)(2,1)S(1)}, bf16[768,1024]{1,0:T(8,128)(2,1)S(1)}) custom-call(bf16[8,8,512,128]{3,2,1,0:T(8,128)(2,1)} %refs_0_.3, bf16[256,1024]{1,0:T(8,128)(2,1)} %refs_1_.3, bf16[256,1024]{1,0:T(8,128)(2,1)} %refs_2_.2, bf16[256,1024]{1,0:T(8,128)(2,1)} %refs_3_.1), custom_call_target="tpu_custom_call" | custom-call | tf_op jit(solution)/shard_map/pallas_call | solution.py:210
  12.3 0.0 collective-permute-done.1.refs_1_
  12.3 0.0 collective-permute-done.2.refs_2_
  12.3 1.5 %collective-permute-done.3.refs_3_ = bf16[16,256]{1,0:T(8,128)(2,1)S(1)} collective-permute-done((bf16[16,256]{1,0:T(8,128)(2,1)S(1)}, bf16[16,256]{1,0:T(8,128)(2,1)S(1)}, u32[]{:S(2)}, u32[]{:S(2)}) %collective-permute-start.3) | collective-permute-done | bytes 8224 | tf_op jit(solution)/shard_map/ppermute | solution.py:232
  13.9 0.4 shard_map.224
  14.2 0.1 collective-permute-start.4
  14.3 0.0 copy-done.9
  14.3 0.1 iota_compare_fusion.1
  14.4 1.3 %collective-permute-done.4 = bf16[32,3072]{1,0:T(8,128)(2,1)S(1)} collective-permute-done((bf16[32,3072]{1,0:T(8,128)(2,1)S(1)}, bf16[32,3072]{1,0:T(8,128)(2,1)S(1)}, u32[]{:S(2)}, u32[]{:S(2)}) %collective-permute-start.4) | collective-permute-done | bytes 196640 | tf_op jit(solution)/shard_map/ppermute | solution.py:227
  15.8 0.1 fusion.41
  15.8 0.1 collective-permute-start.5
  15.9 2.9 %collective-permute-start.6 = (bf16[8,3072]{1,0:T(8,128)(2,1)S(1)}, bf16[8,3072]{1,0:T(8,128)(2,1)S(1)}, u32[]{:S(2)}, u32[]{:S(2)}) collective-permute-start(bf16[8,3072]{1,0:T(8,128)(2,1)S(1)} %get-tuple-element.45), channel_id=1, source_target_pairs={{0,16},{4,20},{8,24},{12,28},{16,0},{20,4},{24,8},{28,12},{1,17},{... | collective-permute-start | bytes 147464 | tf_op jit(solution)/shard_map/ppermute | solution.py:232
  18.8 1.5 %collective-permute-start.7 = (bf16[8,3072]{1,0:T(8,128)(2,1)S(1)}, bf16[8,3072]{1,0:T(8,128)(2,1)S(1)}, u32[]{:S(2)}, u32[]{:S(2)}) collective-permute-start(bf16[8,3072]{1,0:T(8,128)(2,1)S(1)} %get-tuple-element.44), channel_id=1, source_target_pairs={{0,24},{4,28},{8,16},{12,20},{16,8},{20,12},{24,0},{28,4},{1,25},{... | collective-permute-start | bytes 147464 | tf_op jit(solution)/shard_map/ppermute | solution.py:232
  20.3 0.1 slice_reduce_fusion
  20.4 4.7 %shard_map.225 = (bf16[8,8,512,128]{3,2,1,0:T(8,128)(2,1)S(1)}, bf16[1024,2048]{1,0:T(8,128)(2,1)S(1)}) custom-call(bf16[8,8,512,128]{3,2,1,0:T(8,128)(2,1)} %refs_0_.4, bf16[1024,2048]{1,0:T(8,128)(2,1)} %refs_1_.4), custom_call_target="tpu_custom_call" | custom-call | tf_op jit(solution)/shard_map/pallas_call | solution.py:210
  25.1 0.0 copy-start.10
  25.1 0.0 collective-permute-done.5
  25.1 0.0 collective-permute-done.6
  25.2 0.0 collective-permute-done.7
  25.2 0.1 fusion.23
  25.2 0.1 fusion.29
  25.4 0.1 fusion.36
  25.4 2.3 %fusion.34 = f32[8,8,1,512]{3,2,1,0:T(1,128)S(1)} fusion(bf16[8,8,512,128]{3,2,1,0:T(8,128)(2,1)S(1)} %get-tuple-element.31, bf16[8,8,128,1]{2,0,1,3:T(8,128)(2,1)S(1)} %fusion.36), kind=kOutput, calls=%fused_computation.48 | convolution fusion | flops 8388608 | bytes 8536064 | tf_op jit(solution)/shard_map/shd,shld->shl/dot_general | solution.py:532
  27.7 0.6 fusion.3
  28.3 0.0 copy-start.6
  28.3 1.2 %fusion.11 = f32[8,8,1,128]{3,2,1,0:T(1,128)S(1)} fusion(bf16[8,8,512,128]{3,2,1,0:T(8,128)(2,1)S(1)} %get-tuple-element.32, bf16[8,8,512,1]{2,1,0,3:T(8,128)(2,1)S(1)} %fusion.3), kind=kOutput, calls=%fused_computation.16 | convolution fusion | flops 8388608 | bytes 8486912 | tf_op jit(solution)/shard_map/shl,shld->shd/dot_general | solution.py:544
  29.5 0.7 %convolution_convert_fusion.refs_0_ = bf16[8,2048]{1,0:T(8,128)(2,1)S(1)} fusion(bf16[1024,2048]{1,0:T(8,128)(2,1)S(1)} %get-tuple-element.33, bf16[1,8,8,128]{3,2,1,0:T(8,128)(2,1)S(1)} %convert_bitcast_fusion), kind=kOutput, calls=%fused_computation | convolution fusion | flops 33570816 | bytes 4243456 | tf_op jit(solution)/shard_map/dot_general | solution.py:546
  30.1 2.5 %collective-permute-start.10 = (bf16[8,2048]{1,0:T(8,128)(2,1)S(1)}, bf16[8,2048]{1,0:T(8,128)(2,1)S(1)}, u32[]{:S(2)}, u32[]{:S(2)}) collective-permute-start(bf16[8,2048]{1,0:T(8,128)(2,1)S(1)} %convolution_convert_fusion.refs_0_), channel_id=1, source_target_pairs={{0,3},{1,2},{2,1},{3,0},{4,7},{5,6},{6,5},{7,4},{8,11},{9,10},{10,... | collective-permute-start | bytes 98312 | tf_op jit(solution)/shard_map/ppermute | solution.py:237
  32.6 0.5 collective-permute-start.8
  33.1 0.5 collective-permute-start.9
  33.6 0.8 %shard_map.220.picks_ref = bf16[32,512]{1,0:T(8,128)(2,1)S(1)} custom-call(s32[2,8]{1,0:T(2,128)S(1)} %bitcast.52), custom_call_target="tpu_custom_call" | custom-call | tf_op jit(solution)/shard_map/pallas_call | solution.py:168
  34.4 0.0 copy-start.2
  34.4 0.0 copy-start.4
  34.5 0.0 copy-start.7
  34.5 0.0 copy-start
  34.5 0.0 copy-start.5
  34.5 2.7 %shard_map.227.refs_4_ = bf16[4096,640]{1,0:T(8,128)(2,1)S(1)} custom-call(bf16[2048,640]{1,0:T(8,128)(2,1)} %bitcast.55, bf16[2048,640]{1,0:T(8,128)(2,1)} %bitcast.56), custom_call_target="tpu_custom_call" | custom-call | tf_op jit(solution)/shard_map/pallas_call | solution.py:210
  37.2 1.9 %shard_map.228 = (bf16[4096,256]{1,0:T(8,128)(2,1)S(1)}, bf16[256,2048]{1,0:T(8,128)(2,1)S(1)}) custom-call(bf16[2048,256]{1,0:T(8,128)(2,1)} %refs_0_.5, bf16[2048,256]{1,0:T(8,128)(2,1)} %refs_1_.5, bf16[256,2048]{1,0:T(8,128)(2,1)} %refs_2_.3), custom_call_target="tpu_custom_call" | custom-call | tf_op jit(solution)/shard_map/pallas_call | solution.py:210
  39.1 0.0 collective-permute-done.10.refs_3_
  39.1 0.0 collective-permute-done.8.refs_1_
  39.1 0.0 collective-permute-done.9.refs_2_
  39.1 1.0 %shard_map.226 = (f32[8,512]{1,0:T(8,128)S(1)}, bf16[16,2176]{1,0:T(8,128)(2,1)S(1)}, bf16[16,2176]{1,0:T(8,128)(2,1)S(1)}) custom-call(s32[2,8]{1,0:T(2,128)S(1)} %bitcast.53, f32[2,8]{1,0:T(2,128)S(1)} %bitcast.54, bf16[8,2048]{1,0:T(8,128)(2,1)S(1)} %copy-done.2, bf16[8,2048]{1,0:T(8,128)(2,1)S(1)} %convolution_convert_fusion.refs_0_, ...), custom_call_target="tpu_custom_call" | custom-call | tf_op jit(solution)/shard_map/pallas_call | solution.py:366
  40.1 0.1 collective-permute-start.11
  40.2 1.2 %collective-permute-done.11 = bf16[16,2176]{1,0:T(8,128)(2,1)S(1)} collective-permute-done((bf16[16,2176]{1,0:T(8,128)(2,1)S(1)}, bf16[16,2176]{1,0:T(8,128)(2,1)S(1)}, u32[]{:S(2)}, u32[]{:S(2)}) %collective-permute-start.11) | collective-permute-done | bytes 69664 | tf_op jit(solution)/shard_map/ppermute | solution.py:227
  41.5 2.4 %collective-permute-start.14 = (bf16[8,2176]{1,0:T(8,128)(2,1)S(1)}, bf16[8,2176]{1,0:T(8,128)(2,1)S(1)}, u32[]{:S(2)}, u32[]{:S(2)}) collective-permute-start(bf16[8,2176]{1,0:T(8,128)(2,1)S(1)} %pad_maximum_fusion.3), channel_id=1, source_target_pairs={{0,24},{4,28},{8,16},{12,20},{16,8},{20,12},{24,0},{28,4},{1,25},{... | collective-permute-start | bytes 104456 | tf_op jit(solution)/shard_map/ppermute | solution.py:232
  43.9 0.1 collective-permute-start.13
  44.0 2.1 %collective-permute-start.12 = (bf16[8,2176]{1,0:T(8,128)(2,1)S(1)}, bf16[8,2176]{1,0:T(8,128)(2,1)S(1)}, u32[]{:S(2)}, u32[]{:S(2)}) collective-permute-start(bf16[8,2176]{1,0:T(8,128)(2,1)S(1)} %pad_maximum_fusion.1), channel_id=1, source_target_pairs={{0,8},{4,12},{8,0},{12,4},{16,24},{20,28},{24,16},{28,20},{1,9},{5... | collective-permute-start | bytes 104456 | tf_op jit(solution)/shard_map/ppermute | solution.py:232
  46.1 1.2 %collective-permute-done.14.refs_3_ = bf16[8,2176]{1,0:T(8,128)(2,1)S(1)} collective-permute-done((bf16[8,2176]{1,0:T(8,128)(2,1)S(1)}, bf16[8,2176]{1,0:T(8,128)(2,1)S(1)}, u32[]{:S(2)}, u32[]{:S(2)}) %collective-permute-start.14) | collective-permute-done | bytes 34848 | tf_op jit(solution)/shard_map/ppermute | solution.py:232
  47.3 1.5 %collective-permute-done.13.refs_2_ = bf16[8,2176]{1,0:T(8,128)(2,1)S(1)} collective-permute-done((bf16[8,2176]{1,0:T(8,128)(2,1)S(1)}, bf16[8,2176]{1,0:T(8,128)(2,1)S(1)}, u32[]{:S(2)}, u32[]{:S(2)}) %collective-permute-start.13) | collective-permute-done | bytes 34848 | tf_op jit(solution)/shard_map/ppermute | solution.py:232
  48.8 0.0 collective-permute-done.12.refs_1_
  48.8 2.7 %shard_map.229 = bf16[32,16,128]{2,1,0:T(8,128)(2,1)} custom-call(bf16[8,2176]{1,0:T(8,128)(2,1)S(1)} %pad_maximum_fusion.refs_0_, bf16[8,2176]{1,0:T(8,128)(2,1)S(1)} %collective-permute-done.12.refs_1_, bf16[8,2176]{1,0:T(8,128)(2,1)S(1)} %collective-permute-done.13.refs_2_, bf16[8,2176]{1,0:T(8,128)(2,1)S(1)} %collective-permute-done.14.refs_3_, ...), custom_call_target="tpu_custom_call" | custom-call | tf_op jit(solution)/shard_map/pallas_call | solution.py:168
  51.5 4.4 %all-to-all-start = ((bf16[32,16,128]{2,1,0:T(8,128)(2,1)}), bf16[32,16,128]{2,1,0:T(8,128)(2,1)S(1)}, u32[]{:S(2)}, u32[]{:S(2)}) async-start(bf16[32,16,128]{2,1,0:T(8,128)(2,1)} %shard_map.229), calls=%async_computation | async-start | bytes 262144 | tf_op jit(solution)/shard_map/all_to_all | solution.py:562
  55.9 0.6 slice.85
  56.6 0.7 %fusion.30 = bf16[8,1024]{1,0:T(8,128)(2,1)} fusion(f32[8,8]{0,1:T(8,128)S(1)} %add_rsqrt_fusion, bf16[8,3072]{1,0:T(8,128)(2,1)S(1)} %fusion.23), kind=kLoop, calls=%fused_computation.44 | loop fusion | flops 24576 | bytes 33024 | tf_op jit(solution)/shard_map/convert_element_type | solution.py:526
  57.2 7.1 %all-to-all-done.returned_ref = bf16[32,16,128]{2,1,0:T(8,128)(2,1)S(1)} async-done(((bf16[32,16,128]{2,1,0:T(8,128)(2,1)}), bf16[32,16,128]{2,1,0:T(8,128)(2,1)S(1)}, u32[]{:S(2)}, u32[]{:S(2)}) %all-to-all-start) | async-done | bytes 131104 | tf_op jit(solution)/shard_map/all_to_all | solution.py:562
  64.3 0.7 %shard_map.230 = bf16[8,512]{1,0:T(8,128)(2,1)} custom-call(bf16[32,512]{1,0:T(8,128)(2,1)S(1)} %shard_map.220.picks_ref, bf16[32,16,128]{2,1,0:T(8,128)(2,1)S(1)} %all-to-all-done.returned_ref, f32[8,512]{1,0:T(8,128)S(1)} %get-tuple-element.38.middle_ref), custom_call_target="tpu_custom_call" | custom-call | tf_op jit(solution)/shard_map/pallas_call | solution.py:168
  (23 shorter events, 0.2 us)
Async XLA Ops:
  0.6 0.8 %copy-start.1 = (bf16[8,2048]{1,0:T(8,128)(2,1)S(1)}, bf16[8,2048]{1,0:T(8,128)(2,1)}, u32[]{:S(2)}) copy-start(bf16[8,2048]{1,0:T(8,128)(2,1)} %tokens_ref.3) | copy-start | bytes 98308
  1.4 12.5 %copy-start.3 = (f32[2048]{0:T(1024)S(1)}, f32[2048]{0:T(1024)}, u32[]{:S(2)}) copy-start(f32[2048]{0:T(1024)} %param.22) | copy-start | bytes 24580
  1.5 1.3 %collective-permute-start = (bf16[4,8,256]{2,1,0:T(8,128)(2,1)S(1)}, bf16[4,8,256]{2,1,0:T(8,128)(2,1)S(1)}, u32[]{:S(2)}, u32[]{:S(2)}) collective-permute-start(bf16[4,8,256]{2,1,0:T(8,128)(2,1)S(1)} %get-tuple-element.22), channel_id=1, source_target_pairs={{0,4},{4,0},{8,12},{12,8},{16,20},{20,16},{24,28},{28,24},{1,5},{5... | collective-permute-start | bytes 49160 | tf_op jit(solution)/shard_map/ppermute | solution.py:227
  2.8 9.5 %collective-permute-start.1 = (bf16[16,256]{1,0:T(8,128)(2,1)S(1)}, bf16[16,256]{1,0:T(8,128)(2,1)S(1)}, u32[]{:S(2)}, u32[]{:S(2)}) collective-permute-start(bf16[16,256]{1,0:T(8,128)(2,1)S(1)} %get-tuple-element.24), channel_id=1, source_target_pairs={{0,8},{4,12},{8,0},{12,4},{16,24},{20,28},{24,16},{28,20},{1,9},{5... | collective-permute-start | bytes 24584 | tf_op jit(solution)/shard_map/ppermute | solution.py:232
  5.8 6.5 %collective-permute-start.2 = (bf16[16,256]{1,0:T(8,128)(2,1)S(1)}, bf16[16,256]{1,0:T(8,128)(2,1)S(1)}, u32[]{:S(2)}, u32[]{:S(2)}) collective-permute-start(bf16[16,256]{1,0:T(8,128)(2,1)S(1)} %get-tuple-element.25), channel_id=1, source_target_pairs={{0,16},{4,20},{8,24},{12,28},{16,0},{20,4},{24,8},{28,12},{1,17},{... | collective-permute-start | bytes 24584 | tf_op jit(solution)/shard_map/ppermute | solution.py:232
  8.4 5.9 %copy-start.9 = (s32[8]{0:T(128)S(1)}, s32[8]{0:T(128)}, u32[]{:S(2)}) copy-start(s32[8]{0:T(128)} %param.30) | copy-start | bytes 100
  8.4 5.4 %collective-permute-start.3 = (bf16[16,256]{1,0:T(8,128)(2,1)S(1)}, bf16[16,256]{1,0:T(8,128)(2,1)S(1)}, u32[]{:S(2)}, u32[]{:S(2)}) collective-permute-start(bf16[16,256]{1,0:T(8,128)(2,1)S(1)} %get-tuple-element.26), channel_id=1, source_target_pairs={{0,24},{4,28},{8,16},{12,20},{16,8},{20,12},{24,0},{28,4},{1,25},{... | collective-permute-start | bytes 24584 | tf_op jit(solution)/shard_map/ppermute | solution.py:232
  14.2 1.5 %collective-permute-start.4 = (bf16[32,3072]{1,0:T(8,128)(2,1)S(1)}, bf16[32,3072]{1,0:T(8,128)(2,1)S(1)}, u32[]{:S(2)}, u32[]{:S(2)}) collective-permute-start(bf16[32,3072]{1,0:T(8,128)(2,1)S(1)} %get-tuple-element.29), channel_id=1, source_target_pairs={{0,4},{4,0},{8,12},{12,8},{16,20},{20,16},{24,28},{28,24},{1,5},{5... | collective-permute-start | bytes 589832 | tf_op jit(solution)/shard_map/ppermute | solution.py:227
  15.8 9.3 %collective-permute-start.5 = (bf16[8,3072]{1,0:T(8,128)(2,1)S(1)}, bf16[8,3072]{1,0:T(8,128)(2,1)S(1)}, u32[]{:S(2)}, u32[]{:S(2)}) collective-permute-start(bf16[8,3072]{1,0:T(8,128)(2,1)S(1)} %get-tuple-element.43), channel_id=1, source_target_pairs={{0,8},{4,12},{8,0},{12,4},{16,24},{20,28},{24,16},{28,20},{1,9},{5... | collective-permute-start | bytes 147464 | tf_op jit(solution)/shard_map/ppermute | solution.py:232
  15.9 9.2 %collective-permute-start.6 = (bf16[8,3072]{1,0:T(8,128)(2,1)S(1)}, bf16[8,3072]{1,0:T(8,128)(2,1)S(1)}, u32[]{:S(2)}, u32[]{:S(2)}) collective-permute-start(bf16[8,3072]{1,0:T(8,128)(2,1)S(1)} %get-tuple-element.45), channel_id=1, source_target_pairs={{0,16},{4,20},{8,24},{12,28},{16,0},{20,4},{24,8},{28,12},{1,17},{... | collective-permute-start | bytes 147464 | tf_op jit(solution)/shard_map/ppermute | solution.py:232
  18.8 6.4 %collective-permute-start.7 = (bf16[8,3072]{1,0:T(8,128)(2,1)S(1)}, bf16[8,3072]{1,0:T(8,128)(2,1)S(1)}, u32[]{:S(2)}, u32[]{:S(2)}) collective-permute-start(bf16[8,3072]{1,0:T(8,128)(2,1)S(1)} %get-tuple-element.44), channel_id=1, source_target_pairs={{0,24},{4,28},{8,16},{12,20},{16,8},{20,12},{24,0},{28,4},{1,25},{... | collective-permute-start | bytes 147464 | tf_op jit(solution)/shard_map/ppermute | solution.py:232
  20.4 5.0 %copy-start.8 = (f32[128]{0:T(128)S(1)}, f32[128]{0:T(128)}, u32[]{:S(2)}) copy-start(f32[128]{0:T(128)} %param.26) | copy-start | bytes 1540
  25.1 2.6 %copy-start.10 = (f32[8]{0:T(128)S(1)}, f32[8]{0:T(128)}, u32[]{:S(2)}) copy-start(f32[8]{0:T(128)} %param.27) | copy-start | bytes 100
  28.3 5.4 %copy-start.6 = (s32[8,2]{0,1:T(2,128)S(1)}, s32[8,2]{0,1:T(2,128)}, u32[]{:S(2)}) copy-start(s32[8,2]{0,1:T(2,128)} %param.33) | copy-start | bytes 196
  30.1 8.9 %collective-permute-start.10 = (bf16[8,2048]{1,0:T(8,128)(2,1)S(1)}, bf16[8,2048]{1,0:T(8,128)(2,1)S(1)}, u32[]{:S(2)}, u32[]{:S(2)}) collective-permute-start(bf16[8,2048]{1,0:T(8,128)(2,1)S(1)} %convolution_convert_fusion.refs_0_), channel_id=1, source_target_pairs={{0,3},{1,2},{2,1},{3,0},{4,7},{5,6},{6,5},{7,4},{8,11},{9,10},{10,... | collective-permute-start | bytes 98312 | tf_op jit(solution)/shard_map/ppermute | solution.py:237
  32.6 6.5 %collective-permute-start.8 = (bf16[8,2048]{1,0:T(8,128)(2,1)S(1)}, bf16[8,2048]{1,0:T(8,128)(2,1)S(1)}, u32[]{:S(2)}, u32[]{:S(2)}) collective-permute-start(bf16[8,2048]{1,0:T(8,128)(2,1)S(1)} %convolution_convert_fusion.refs_0_), channel_id=1, source_target_pairs={{0,1},{1,0},{2,3},{3,2},{4,5},{5,4},{6,7},{7,6},{8,9},{9,8},{10,11... | collective-permute-start | bytes 98312 | tf_op jit(solution)/shard_map/ppermute | solution.py:237
  33.1 6.0 %collective-permute-start.9 = (bf16[8,2048]{1,0:T(8,128)(2,1)S(1)}, bf16[8,2048]{1,0:T(8,128)(2,1)S(1)}, u32[]{:S(2)}, u32[]{:S(2)}) collective-permute-start(bf16[8,2048]{1,0:T(8,128)(2,1)S(1)} %convolution_convert_fusion.refs_0_), channel_id=1, source_target_pairs={{0,2},{1,3},{2,0},{3,1},{4,6},{5,7},{6,4},{7,5},{8,10},{9,11},{10,... | collective-permute-start | bytes 98312 | tf_op jit(solution)/shard_map/ppermute | solution.py:237
  34.4 4.7 %copy-start.2 = (bf16[8,2048]{1,0:T(8,128)(2,1)S(1)}, bf16[8,2048]{1,0:T(8,128)(2,1)}, u32[]{:S(2)}) copy-start(bf16[8,2048]{1,0:T(8,128)(2,1)} %tokens_ref.3) | copy-start | bytes 98308
  34.4 4.7 %copy-start.4 = (f32[2048]{0:T(1024)S(1)}, f32[2048]{0:T(1024)}, u32[]{:S(2)}) copy-start(f32[2048]{0:T(1024)} %param.32) | copy-start | bytes 24580
  34.5 4.7 %copy-start.7 = (f32[8,2]{0,1:T(2,128)S(1)}, f32[8,2]{0,1:T(2,128)}, u32[]{:S(2)}) copy-start(f32[8,2]{0,1:T(2,128)} %param.34) | copy-start | bytes 196
  34.5 14.4 %copy-start = (bf16[1,640,2048]{2,1,0:T(8,128)(2,1)S(1)}, bf16[1,640,2048]{2,1,0:T(8,128)(2,1)}, u32[]{:S(2)}) copy-start(bf16[1,640,2048]{2,1,0:T(8,128)(2,1)} %param.37) | copy-start | bytes 7864324
  34.5 14.3 %copy-start.5 = (f32[2048]{0:T(1024)S(1)}, f32[2048]{0:T(1024)}, u32[]{:S(2)}) copy-start(f32[2048]{0:T(1024)} %param.41) | copy-start | bytes 24580
  40.1 1.3 %collective-permute-start.11 = (bf16[16,2176]{1,0:T(8,128)(2,1)S(1)}, bf16[16,2176]{1,0:T(8,128)(2,1)S(1)}, u32[]{:S(2)}, u32[]{:S(2)}) collective-permute-start(bf16[16,2176]{1,0:T(8,128)(2,1)S(1)} %get-tuple-element.35), channel_id=1, source_target_pairs={{0,4},{4,0},{8,12},{12,8},{16,20},{20,16},{24,28},{28,24},{1,5},{5... | collective-permute-start | bytes 208904 | tf_op jit(solution)/shard_map/ppermute | solution.py:227
  41.5 5.8 %collective-permute-start.14 = (bf16[8,2176]{1,0:T(8,128)(2,1)S(1)}, bf16[8,2176]{1,0:T(8,128)(2,1)S(1)}, u32[]{:S(2)}, u32[]{:S(2)}) collective-permute-start(bf16[8,2176]{1,0:T(8,128)(2,1)S(1)} %pad_maximum_fusion.3), channel_id=1, source_target_pairs={{0,24},{4,28},{8,16},{12,20},{16,8},{20,12},{24,0},{28,4},{1,25},{... | collective-permute-start | bytes 104456 | tf_op jit(solution)/shard_map/ppermute | solution.py:232
  43.9 4.9 %collective-permute-start.13 = (bf16[8,2176]{1,0:T(8,128)(2,1)S(1)}, bf16[8,2176]{1,0:T(8,128)(2,1)S(1)}, u32[]{:S(2)}, u32[]{:S(2)}) collective-permute-start(bf16[8,2176]{1,0:T(8,128)(2,1)S(1)} %pad_maximum_fusion.2), channel_id=1, source_target_pairs={{0,16},{4,20},{8,24},{12,28},{16,0},{20,4},{24,8},{28,12},{1,17},{... | collective-permute-start | bytes 104456 | tf_op jit(solution)/shard_map/ppermute | solution.py:232
  44.0 4.8 %collective-permute-start.12 = (bf16[8,2176]{1,0:T(8,128)(2,1)S(1)}, bf16[8,2176]{1,0:T(8,128)(2,1)S(1)}, u32[]{:S(2)}, u32[]{:S(2)}) collective-permute-start(bf16[8,2176]{1,0:T(8,128)(2,1)S(1)} %pad_maximum_fusion.1), channel_id=1, source_target_pairs={{0,8},{4,12},{8,0},{12,4},{16,24},{20,28},{24,16},{28,20},{1,9},{5... | collective-permute-start | bytes 104456 | tf_op jit(solution)/shard_map/ppermute | solution.py:232
  51.5 12.8 %all-to-all-start = ((bf16[32,16,128]{2,1,0:T(8,128)(2,1)}), bf16[32,16,128]{2,1,0:T(8,128)(2,1)S(1)}, u32[]{:S(2)}, u32[]{:S(2)}) async-start(bf16[32,16,128]{2,1,0:T(8,128)(2,1)} %shard_map.229), calls=%async_computation | async-start | bytes 262144 | tf_op jit(solution)/shard_map/all_to_all | solution.py:562

commit v3 on v2

--- a/solution.py
+++ b/solution.py
@@ -175,7 +175,7 @@
     )(*arrays)
 
 
-def stage(*groups):
+def stage(*groups, scalars=(), outs=(), work=None):
     plan, shapes = [], []
     for target, group in enumerate(groups):
         offset = 0
@@ -191,7 +191,9 @@
     total = sum(count for *_, count in plan)
 
     def kernel(*refs):
-        sources, targets, sems = refs[: len(arrays)], refs[len(arrays) : -1], refs[-1]
+        scalar_refs, refs = refs[: len(scalars)], refs[len(scalars) :]
+        sources, sems = refs[: len(arrays)], refs[-1]
+        targets = refs[len(arrays) : len(arrays) + len(groups)]
         copies = []
         for source, (target, offset, rows, count) in zip(sources, plan):
             for i in range(count):
@@ -204,15 +206,96 @@
                 )
         for copy in copies:
             copy.start()
+        if work is not None:
+            work(*scalar_refs, *refs[len(arrays) + len(groups) : -1])
         for copy in copies:
             copy.wait()
 
     return pl.pallas_call(
         kernel,
-        out_shape=shapes,
-        in_specs=[pl.BlockSpec(memory_space=pltpu.HBM) for _ in arrays],
-        out_specs=in_vmem(len(groups)),
+        out_shape=shapes + [jax.ShapeDtypeStruct(shape, dtype) for shape, dtype in outs],
+        in_specs=[pl.BlockSpec(memory_space=pltpu.SMEM)] * len(scalars)
+        + [pl.BlockSpec(memory_space=pltpu.HBM) for _ in arrays],
+        out_specs=in_vmem(len(groups) + len(outs)),
         scratch_shapes=[pltpu.SemaphoreType.DMA((total,))],
+        compiler_params=pltpu.CompilerParams(vmem_limit_bytes=1 << 20),
+    )(*scalars, *[pltpu.with_memory_space_constraint(array, pltpu.HBM) for array in arrays])
+
+
+def stage_keys(keys, *arrays):
+    seqs, heads, slots, size = keys.shape
+    rows = [array.shape[0] for array in arrays]
+
+    def kernel(keys_ref, *refs):
+        array_refs = refs[: len(arrays)]
+        turned_ref, stacked_ref, scratch, key_sems, array_sems = refs[len(arrays) :]
+        key_copies = [
+            pltpu.make_async_copy(keys_ref.at[s], scratch.at[s], key_sems.at[s])
+            for s in range(seqs)
+        ]
+        array_copies = [
+            pltpu.make_async_copy(
+                ref, stacked_ref.at[pl.ds(sum(rows[:i]), rows[i])], array_sems.at[i]
+            )
+            for i, ref in enumerate(array_refs)
+        ]
+        for copy in key_copies + array_copies:
+            copy.start()
+        for s in range(seqs):
+            key_copies[s].wait()
+            for h in range(heads):
+                turned_ref[s, h] = scratch[s, h].T
+        for copy in array_copies:
+            copy.wait()
+
+    return pl.pallas_call(
+        kernel,
+        out_shape=[
+            pltpu.VMEM((seqs, heads, size, slots), keys.dtype),
+            pltpu.VMEM((sum(rows),) + arrays[0].shape[1:], arrays[0].dtype),
+        ],
+        in_specs=[pl.BlockSpec(memory_space=pltpu.HBM)] * (1 + len(arrays)),
+        out_specs=in_vmem(2),
+        scratch_shapes=[
+            pltpu.VMEM(keys.shape, keys.dtype),
+            pltpu.SemaphoreType.DMA((seqs,)),
+            pltpu.SemaphoreType.DMA((len(arrays),)),
+        ],
+        compiler_params=pltpu.CompilerParams(vmem_limit_bytes=16 << 20),
+    )(*[pltpu.with_memory_space_constraint(array, pltpu.HBM) for array in (keys, *arrays)])
+
+
+def stage_beside(*pairs):
+    def kernel(*refs):
+        sources, targets, sems = refs[: 2 * len(pairs)], refs[2 * len(pairs) : -1], refs[-1]
+        copies = []
+        for n, target in enumerate(targets):
+            rows, width = sources[2 * n].shape
+            pieces = 4 if rows % 64 == 0 else 1
+            for k in range(2):
+                for i in range(pieces):
+                    part = pl.ds(i * (rows // pieces), rows // pieces)
+                    copies.append(
+                        pltpu.make_async_copy(
+                            sources[2 * n + k].at[part],
+                            target.at[part, pl.ds(k * width, width)],
+                            sems.at[len(copies)],
+                        )
+                    )
+        for copy in copies:
+            copy.start()
+        for copy in copies:
+            copy.wait()
+
+    arrays = [array for pair in pairs for array in pair]
+    return pl.pallas_call(
+        kernel,
+        out_shape=[
+            pltpu.VMEM((pair[0].shape[0], 2 * pair[0].shape[1]), pair[0].dtype) for pair in pairs
+        ],
+        in_specs=[pl.BlockSpec(memory_space=pltpu.HBM)] * len(arrays),
+        out_specs=in_vmem(len(pairs)),
+        scratch_shapes=[pltpu.SemaphoreType.DMA((8 * len(pairs),))],
         compiler_params=pltpu.CompilerParams(vmem_limit_bytes=1 << 20),
     )(*[pltpu.with_memory_space_constraint(array, pltpu.HBM) for array in arrays])
 
@@ -241,38 +324,28 @@
     return pl.multiple_of(index * size, size)
 
 
-def split_tokens(tokens):
+def row_scales(tokens):
+    def kernel(tokens_ref, scale_ref):
+        stream = tokens_ref[...].astype(jnp.float32)
+        mean_square = jnp.mean(stream * stream, axis=-1, keepdims=True)
+        scale_ref[...] = jnp.broadcast_to(lax.rsqrt(mean_square + epsilon), scale_ref.shape)
+
+    return call(kernel, [((tokens.shape[0], LANES), jnp.float32)], tokens)[0]
+
+
+def knit(tokens, came):
     rows, width = tokens.shape
     count = lax.axis_size("ep")
     features = width // count
     half = count // 2
 
-    def kernel(tokens_ref, away_ref, kept_ref, scale_ref):
+    def kernel(tokens_ref, came_ref, *outs):
         high, low = place()
-        for step in range(half):
-            for target, side in ((kept_ref, low), (away_ref, 1 - low)):
-                column = aligned(2 * (high ^ step) + side, features)
-                target[step] = tokens_ref[:, pl.ds(column, features)]
-        stream = tokens_ref[...].astype(jnp.float32)
-        mean_square = jnp.mean(stream * stream, axis=-1, keepdims=True)
-        scale_ref[...] = jnp.broadcast_to(lax.rsqrt(mean_square + epsilon), scale_ref.shape)
-
-    shape = (half, rows, features)
-    return call(
-        kernel,
-        [(shape, tokens.dtype), (shape, tokens.dtype), ((rows, LANES), jnp.float32)],
-        tokens,
-    )
-
-
-def knit(kept, came):
-    half, rows, width = kept.shape
-
-    def kernel(kept_ref, came_ref, *outs):
         for step, out_ref in enumerate(outs):
-            out_ref[...] = jnp.concatenate([kept_ref[step], came_ref[step]], axis=0)
-
-    return call(kernel, [((2 * rows, width), kept.dtype)] * half, kept, came)
+            part = pl.ds(aligned(2 * (high ^ step) + low, features), features)
+            out_ref[...] = jnp.concatenate([tokens_ref[:, part], came_ref[:, part]], axis=0)
+
+    return call(kernel, [((2 * rows, features), tokens.dtype)] * half, tokens, came)
 
 
 def project(parts, gain, weights, parts_out):
@@ -316,27 +389,11 @@
     return chosen
 
 
-def dispatch(ids, weights, tokens, attn_parts, mix_gain, capacity):
-    rows, width = tokens.shape
-    count, tp_size = lax.axis_size("ep"), lax.axis_size("tp")
-    half = count // 2
-    col_width = width // tp_size
+def plan_sends(capacity):
+    half = lax.axis_size("ep") // 2
     slots = half * capacity
-    terms = len(attn_parts)
-
-    def kernel(ids_ref, weights_ref, tokens_ref, *refs):
-        part_refs, gain_ref = refs[:terms], refs[terms]
-        middle_ref, kept_ref, away_ref, scratch = refs[terms + 1 :]
-        proj = part_refs[0][...].astype(jnp.float32)
-        for ref in part_refs[1:]:
-            proj = proj + ref[...].astype(jnp.float32)
-        middle = (tokens_ref[...].astype(jnp.float32) + proj).astype(jnp.bfloat16)
-        wide = middle.astype(jnp.float32)
-        scratch[...] = wide
-        column = aligned(lax.axis_index("tp"), col_width)
-        middle_ref[...] = scratch[:, pl.ds(column, col_width)]
-        mean_square = jnp.mean(wide * wide, axis=-1, keepdims=True)
-        normed = (wide * lax.rsqrt(mean_square + epsilon) * gain_ref[...]).astype(jnp.bfloat16)
+
+    def kernel(ids_ref, weights_ref, picks_ref, notes_ref):
         high, low = place()
         line = lax.broadcasted_iota(jnp.int32, (2 * slots, LANES), 0)
         lane = lax.broadcasted_iota(jnp.int32, (2 * slots, LANES), 1)
@@ -351,16 +408,41 @@
             share = jnp.where(here, weights_ref[k, b], share)
             if k == 0:
                 first = jnp.where(here, 1.0, first)
-        outbox = jnp.dot(
-            picks[:, :rows].astype(jnp.bfloat16), normed, preferred_element_type=jnp.float32
-        ).astype(jnp.bfloat16)
         upper = share.astype(jnp.bfloat16).astype(jnp.float32)
         notes = jnp.where(lane == 0, upper, jnp.where(lane == 1, share - upper, first))
-        notes = notes.astype(jnp.bfloat16)
+        picks_ref[...] = picks.astype(jnp.bfloat16)
+        notes_ref[...] = notes.astype(jnp.bfloat16)
+
+    shape = (2 * slots, LANES)
+    return [(shape, jnp.bfloat16), (shape, jnp.bfloat16)], kernel
+
+
+def dispatch(picks, notes, tokens, attn_parts, mix_gain):
+    rows, width = tokens.shape
+    col_width = width // lax.axis_size("tp")
+    slots = picks.shape[0] // 2
+    terms = len(attn_parts)
+
+    def kernel(picks_ref, notes_ref, tokens_ref, *refs):
+        part_refs, gain_ref = refs[:terms], refs[terms]
+        middle_ref, kept_ref, away_ref, scratch = refs[terms + 1 :]
+        proj = part_refs[0][...].astype(jnp.float32)
+        for ref in part_refs[1:]:
+            proj = proj + ref[...].astype(jnp.float32)
+        middle = (tokens_ref[...].astype(jnp.float32) + proj).astype(jnp.bfloat16)
+        wide = middle.astype(jnp.float32)
+        scratch[...] = wide
+        column = aligned(lax.axis_index("tp"), col_width)
+        middle_ref[...] = scratch[:, pl.ds(column, col_width)]
+        mean_square = jnp.mean(wide * wide, axis=-1, keepdims=True)
+        normed = (wide * lax.rsqrt(mean_square + epsilon) * gain_ref[...]).astype(jnp.bfloat16)
+        outbox = jnp.dot(
+            picks_ref[:, :rows], normed, preferred_element_type=jnp.float32
+        ).astype(jnp.bfloat16)
         kept_ref[:, :width] = outbox[:slots]
         away_ref[:, :width] = outbox[slots:]
-        kept_ref[:, width:] = notes[:slots]
-        away_ref[:, width:] = notes[slots:]
+        kept_ref[:, width:] = notes_ref[:slots]
+        away_ref[:, width:] = notes_ref[slots:]
 
     shape = (slots, width + LANES)
     return pl.pallas_call(
@@ -370,11 +452,11 @@
             jax.ShapeDtypeStruct(shape, jnp.bfloat16),
             jax.ShapeDtypeStruct(shape, jnp.bfloat16),
         ],
-        in_specs=[pl.BlockSpec(memory_space=pltpu.SMEM)] * 2 + in_vmem(terms + 2),
+        in_specs=in_vmem(terms + 4),
         out_specs=in_vmem(3),
         scratch_shapes=[pltpu.VMEM((rows, width), jnp.float32)],
         compiler_params=pltpu.CompilerParams(vmem_limit_bytes=8 << 20),
-    )(ids, weights, tokens, *attn_parts, mix_gain.reshape(1, -1))
+    )(picks, notes, tokens, *attn_parts, mix_gain.reshape(1, -1))
 
 
 def experts_apply(parts, gate_up, down, side_in, side_back, branch_gate, capacity):
@@ -393,13 +475,16 @@
         logit = jnp.sum(lines.astype(jnp.float32) * branch_ref[...], axis=1, keepdims=True)
         switch = notes[:, 2:3] * jax.nn.sigmoid(logit)
 
-        def hidden_of(ref):
-            gate_pre = jnp.dot(lines, ref[:width, :], preferred_element_type=jnp.float32)
-            up_pre = jnp.dot(lines, ref[width:, :], preferred_element_type=jnp.float32)
+        def hidden_of(gate_pre, up_pre):
             return (jax.nn.silu(gate_pre) * up_pre).astype(jnp.bfloat16)
 
-        hidden = hidden_of(gate_up_ref)
-        side_hidden = hidden_of(side_in_ref)
+        both = jnp.dot(lines, gate_up_ref[...], preferred_element_type=jnp.float32)
+        units = both.shape[1] // 2
+        hidden = hidden_of(both[:, :units], both[:, units:])
+        side_hidden = hidden_of(
+            jnp.dot(lines, side_in_ref[:width, :], preferred_element_type=jnp.float32),
+            jnp.dot(lines, side_in_ref[width:, :], preferred_element_type=jnp.float32),
+        )
         high, low = place()
         for t in range(tp_size):
             columns = slice(t * col_width, (t + 1) * col_width)
@@ -505,11 +590,11 @@
     top_count = route_ids.shape[1]
     capacity = max(2, 2 * top_count * seq_count // experts)
 
-    away, kept, scales = split_tokens(tokens)
-    came = pair_move(away)
-    parts = knit(kept, came)
+    came = pair_move(tokens)
+    scales = row_scales(tokens)
+    parts = knit(tokens, came)
     parts = [parts[0]] + [far_move(parts[step], step) for step in range(1, half)]
-    key_cache, weights = stage([key_cache], [query_weight, key_weight, value_weight])
+    turned_keys, weights = stage_keys(key_cache, query_weight, key_weight, value_weight)
     away, kept = project(parts, attn_gain, weights, 3)
     came = pair_move(away)
     both = kept + came.astype(jnp.float32)
@@ -527,9 +612,11 @@
     query_heads = rms_scale(
         query_rows.astype(jnp.float32).reshape(seq_count, heads_local, DH), query_gain
     ).astype(jnp.bfloat16)
-    value_cache, out_weight = stage([value_cache], [out_weight])
-
-    scores = jnp.einsum("shd,shld->shl", query_heads, key_cache, preferred_element_type=jnp.float32)
+    (value_cache,) = stage([value_cache])
+
+    scores = jnp.einsum(
+        "shd,shdl->shl", query_heads, turned_keys, preferred_element_type=jnp.float32
+    )
     scores = scores * DH ** (-0.5) + stick_bias[None, :, None]
     positions = jnp.arange(cache_slots, dtype=jnp.int32)
     visible = positions[None, None, :] < lengths[:, None, None]
@@ -546,16 +633,22 @@
     attn_part = jnp.dot(attended, out_weight, preferred_element_type=jnp.float32)
     attn_part = attn_part.astype(jnp.bfloat16)
     attn_parts = [attn_part] + [tp_move(attn_part, turn) for turn in range(1, tp_size)]
-    side_in, side_back = stage([side_gate, side_up], [side_down])
-
-    ids, weights_t = route_ids.T, route_weights.T
-    middle, kept, away = dispatch(ids, weights_t, tokens, attn_parts, mix_gain, capacity)
+    ids = route_ids.T
+    plan_outs, plan_work = plan_sends(capacity)
+    side_in, side_back, picks, notes = stage(
+        [side_gate, side_up],
+        [side_down],
+        scalars=(ids, route_weights.T),
+        outs=plan_outs,
+        work=plan_work,
+    )
+    middle, kept, away = dispatch(picks, notes, tokens, attn_parts, mix_gain)
     came = pair_move(away)
     kept = kept.reshape(half, capacity, -1)
     came = came.reshape(half, capacity, -1)
     parts = [jnp.concatenate([kept[step], came[step]], axis=0) for step in range(half)]
     parts = [parts[0]] + [far_move(parts[step], step) for step in range(1, half)]
-    (gate_up,) = stage([expert_gate[0], expert_up[0]])
+    (gate_up,) = stage_beside((expert_gate[0], expert_up[0]))
     blocks = experts_apply(
         parts, gate_up, expert_down[0], side_in, side_back, branch_gate, capacity
     )

time: 65.3 us -> 63.8 us (0.977)
  Pallas kernels: 18.8 us -> 17.6 us
  matrix products: 4.68 us -> 3.59 us
  waiting for transfers between devices: 14.7 us -> 15.5 us
    dot_general x1, matrix products: 2.26 us -> 1.19 us  [fast_layer(): jnp.einsum('shd,shdl->shl', query_heads, turned_keys, preferred_element_t...]
    pallas_call x1, Pallas kernels: 0.95 us -> 0.28 us  [dispatch(): pl.pallas_call(kernel, out_shape=[jax.ShapeDtypeStruct((rows, col_width),...]
  transfers between devices with their start and end apart: 16 -> 16, of which waited for: 7 -> 9; matrix products, arithmetic and copies ran while one was open for 2% -> 2% of each run, Pallas kernels for 21% -> 21%
where the time goes in v3:
time: 63.8 us; the launch traced here: 63.5 us
  starting transfers between devices  22.7 us (36%)
  Pallas kernels  17.6 us (28%)
  waiting for transfers between devices  15.5 us (24%)
  matrix products  3.59 us (6%)
  local copies, waits for them, and re-layouts  2.01 us (3%)
  other arithmetic  1.16 us (2%)
  between operations  0.94 us (1%)
    ppermute x9, starting transfers between devices, far_move(): return lax.ppermute(values, 'ep', [(i, i ^ 2 * step) for i in range(count)])  14.6 us
    all_to_all x1, waiting for transfers between devices, fast_layer(): lax.all_to_all(blocks, ('ep', 'tp'), split_axis=0, concat_axis=0, tiled=T...  7.08 us
    pallas_call x2, Pallas kernels, stage(): pl.pallas_call(kernel, out_shape=shapes + [jax.ShapeDtypeStruct(shape, dt...  5.93 us
    ppermute x9, waiting for transfers between devices, far_move(): return lax.ppermute(values, 'ep', [(i, i ^ 2 * step) for i in range(count)])  4.81 us
    pallas_call x6, Pallas kernels, call(): pl.pallas_call(kernel, out_shape=[jax.ShapeDtypeStruct(shape, dtype) for...  4.74 us
    pallas_call x1, Pallas kernels, stage_keys(): pl.pallas_call(kernel, out_shape=[pltpu.VMEM((seqs, heads, size, slots),...  4.13 us
    all_to_all x1, starting transfers between devices, fast_layer(): lax.all_to_all(blocks, ('ep', 'tp'), split_axis=0, concat_axis=0, tiled=T...  3.91 us
    ppermute x3, waiting for transfers between devices, pair_move(): return lax.ppermute(values, 'ep', [(i, i ^ 1) for i in range(count)])  3.63 us
  transfers between devices with their start and end apart: 16, of which 9 were waited for; matrix products, arithmetic and copies ran while one was open for 2% of the time, Pallas kernels for 21%

profile of v3, /device:TPU:0, one launch (start us, length us, event | category | flops | bytes accessed | tf_op | source)
XLA Modules:
  0.0 63.5 jit_solution(1020620850240519796)
XLA Ops:
  0.6 0.6 collective-permute-start
  1.2 1.1 %collective-permute-done.came_ref = bf16[8,2048]{1,0:T(8,128)(2,1)S(1)} collective-permute-done((bf16[8,2048]{1,0:T(8,128)(2,1)}, bf16[8,2048]{1,0:T(8,128)(2,1)S(1)}, u32[]{:S(2)}, u32[]{:S(2)}) %collective-permute-start) | collective-permute-done | bytes 32800 | tf_op jit(solution)/shard_map/ppermute | solution.py:310
  2.3 0.8 %copy-done.1 = bf16[8,2048]{1,0:T(8,128)(2,1)S(1)} copy-done((bf16[8,2048]{1,0:T(8,128)(2,1)S(1)}, bf16[8,2048]{1,0:T(8,128)(2,1)}, u32[]{:S(2)}) %copy-start.1) | copy-done | bytes 32792
  3.0 3.0 %collective-permute-start.1 = (bf16[16,256]{1,0:T(8,128)(2,1)S(1)}, bf16[16,256]{1,0:T(8,128)(2,1)S(1)}, u32[]{:S(2)}, u32[]{:S(2)}) collective-permute-start(bf16[16,256]{1,0:T(8,128)(2,1)S(1)} %get-tuple-element.21), channel_id=1, source_target_pairs={{0,8},{4,12},{8,0},{12,4},{16,24},{20,28},{24,16},{28,20},{1,9},{5... | collective-permute-start | bytes 24584 | tf_op jit(solution)/shard_map/ppermute | solution.py:315
  6.0 2.6 %collective-permute-start.2 = (bf16[16,256]{1,0:T(8,128)(2,1)S(1)}, bf16[16,256]{1,0:T(8,128)(2,1)S(1)}, u32[]{:S(2)}, u32[]{:S(2)}) collective-permute-start(bf16[16,256]{1,0:T(8,128)(2,1)S(1)} %get-tuple-element.22), channel_id=1, source_target_pairs={{0,16},{4,20},{8,24},{12,28},{16,0},{20,4},{24,8},{28,12},{1,17},{... | collective-permute-start | bytes 24584 | tf_op jit(solution)/shard_map/ppermute | solution.py:315
  8.6 0.0 collective-permute-start.3
  8.6 0.1 shard_map.225
  8.7 4.1 %shard_map.223 = (bf16[8,8,128,512]{3,2,1,0:T(8,128)(2,1)S(1)}, bf16[768,1024]{1,0:T(8,128)(2,1)S(1)}) custom-call(bf16[8,8,512,128]{3,2,1,0:T(8,128)(2,1)} %keys_ref.1, bf16[256,1024]{1,0:T(8,128)(2,1)} %refs_0_.2, bf16[256,1024]{1,0:T(8,128)(2,1)} %refs_1_.1, bf16[256,1024]{1,0:T(8,128)(2,1)} %refs_2_.3), custom_call_target="tpu_custom_call" | custom-call | tf_op jit(solution)/shard_map/pallas_call | solution.py:251
  12.8 0.0 collective-permute-done.1.refs_1_
  12.8 0.0 collective-permute-done.2.refs_2_
  12.9 1.2 %collective-permute-done.3.refs_3_ = bf16[16,256]{1,0:T(8,128)(2,1)S(1)} collective-permute-done((bf16[16,256]{1,0:T(8,128)(2,1)S(1)}, bf16[16,256]{1,0:T(8,128)(2,1)S(1)}, u32[]{:S(2)}, u32[]{:S(2)}) %collective-permute-start.3) | collective-permute-done | bytes 8224 | tf_op jit(solution)/shard_map/ppermute | solution.py:315
  14.1 0.0 copy-done.3
  14.1 0.4 shard_map.224
  14.4 0.1 collective-permute-start.4
  14.5 0.0 copy-done.10
  14.5 0.1 iota_compare_fusion.1
  14.6 1.3 %collective-permute-done.4 = bf16[32,3072]{1,0:T(8,128)(2,1)S(1)} collective-permute-done((bf16[32,3072]{1,0:T(8,128)(2,1)S(1)}, bf16[32,3072]{1,0:T(8,128)(2,1)S(1)}, u32[]{:S(2)}, u32[]{:S(2)}) %collective-permute-start.4) | collective-permute-done | bytes 196640 | tf_op jit(solution)/shard_map/ppermute | solution.py:310
  16.0 0.1 fusion.41
  16.0 0.1 collective-permute-start.5
  16.1 3.2 %collective-permute-start.6 = (bf16[8,3072]{1,0:T(8,128)(2,1)S(1)}, bf16[8,3072]{1,0:T(8,128)(2,1)S(1)}, u32[]{:S(2)}, u32[]{:S(2)}) collective-permute-start(bf16[8,3072]{1,0:T(8,128)(2,1)S(1)} %get-tuple-element.39), channel_id=1, source_target_pairs={{0,16},{4,20},{8,24},{12,28},{16,0},{20,4},{24,8},{28,12},{1,17},{... | collective-permute-start | bytes 147464 | tf_op jit(solution)/shard_map/ppermute | solution.py:315
  19.3 1.2 %collective-permute-start.7 = (bf16[8,3072]{1,0:T(8,128)(2,1)S(1)}, bf16[8,3072]{1,0:T(8,128)(2,1)S(1)}, u32[]{:S(2)}, u32[]{:S(2)}) collective-permute-start(bf16[8,3072]{1,0:T(8,128)(2,1)S(1)} %get-tuple-element.38), channel_id=1, source_target_pairs={{0,24},{4,28},{8,16},{12,20},{16,8},{20,12},{24,0},{28,4},{1,25},{... | collective-permute-start | bytes 147464 | tf_op jit(solution)/shard_map/ppermute | solution.py:315
  20.5 0.1 slice_reduce_fusion
  20.6 3.5 %shard_map.226 = bf16[8,8,512,128]{3,2,1,0:T(8,128)(2,1)S(1)} custom-call(bf16[8,8,512,128]{3,2,1,0:T(8,128)(2,1)} %refs_0_.3), custom_call_target="tpu_custom_call" | custom-call | tf_op jit(solution)/shard_map/pallas_call | solution.py:214
  24.1 0.0 copy-start.11
  24.1 0.0 collective-permute-done.5
  24.1 0.0 collective-permute-done.6
  24.1 1.1 %collective-permute-done.7 = bf16[8,3072]{1,0:T(8,128)(2,1)S(1)} collective-permute-done((bf16[8,3072]{1,0:T(8,128)(2,1)S(1)}, bf16[8,3072]{1,0:T(8,128)(2,1)S(1)}, u32[]{:S(2)}, u32[]{:S(2)}) %collective-permute-start.7) | collective-permute-done | bytes 49184 | tf_op jit(solution)/shard_map/ppermute | solution.py:315
  25.2 0.1 fusion.23
  25.3 0.1 fusion.29
  25.4 0.0 copy-done.9
  25.4 0.1 fusion.36
  25.5 1.2 %fusion.34 = f32[8,8,1,512]{3,2,1,0:T(1,128)S(1)} fusion(bf16[8,8,128,512]{3,2,1,0:T(8,128)(2,1)S(1)} %get-tuple-element.27, bf16[8,8,128,1]{2,0,1,3:T(8,128)(2,1)S(1)} %fusion.36), kind=kOutput, calls=%fused_computation.48 | convolution fusion | flops 8388608 | bytes 8536064 | tf_op jit(solution)/shard_map/shd,shdl->shl/dot_general | solution.py:617
  26.7 0.0 copy-done.11
  26.7 0.6 fusion.3
  27.2 1.2 %fusion.11 = f32[8,8,1,128]{3,2,1,0:T(1,128)S(1)} fusion(bf16[8,8,512,128]{3,2,1,0:T(8,128)(2,1)S(1)} %shard_map.226, bf16[8,8,512,1]{2,1,0,3:T(8,128)(2,1)S(1)} %fusion.3), kind=kOutput, calls=%fused_computation.16 | convolution fusion | flops 8388608 | bytes 8486912 | tf_op jit(solution)/shard_map/shl,shld->shd/dot_general | solution.py:631
  28.4 0.4 copy-done.8
  28.9 0.7 %convolution_convert_fusion.refs_0_ = bf16[8,2048]{1,0:T(8,128)(2,1)S(1)} fusion(bf16[1024,2048]{1,0:T(8,128)(2,1)S(1)} %copy-done.8, bf16[1,8,8,128]{3,2,1,0:T(8,128)(2,1)S(1)} %convert_bitcast_fusion), kind=kOutput, calls=%fused_computation | convolution fusion | flops 33570816 | bytes 4243456 | tf_op jit(solution)/shard_map/dot_general | solution.py:633
  29.5 2.5 %collective-permute-start.10 = (bf16[8,2048]{1,0:T(8,128)(2,1)S(1)}, bf16[8,2048]{1,0:T(8,128)(2,1)S(1)}, u32[]{:S(2)}, u32[]{:S(2)}) collective-permute-start(bf16[8,2048]{1,0:T(8,128)(2,1)S(1)} %convolution_convert_fusion.refs_0_), channel_id=1, source_target_pairs={{0,3},{1,2},{2,1},{3,0},{4,7},{5,6},{6,5},{7,4},{8,11},{9,10},{10,... | collective-permute-start | bytes 98312 | tf_op jit(solution)/shard_map/ppermute | solution.py:320
  32.0 0.5 collective-permute-start.8
  32.5 0.5 collective-permute-start.9
  33.0 0.0 copy-done.6
  33.0 0.8 %shard_map.220.picks_ref = bf16[32,512]{1,0:T(8,128)(2,1)S(1)} custom-call(s32[2,8]{1,0:T(2,128)S(1)} %bitcast.52), custom_call_target="tpu_custom_call" | custom-call | tf_op jit(solution)/shard_map/pallas_call | solution.py:168
  33.8 2.5 %shard_map.228.refs_4_ = bf16[2048,1280]{1,0:T(8,128)(2,1)S(1)} custom-call(bf16[2048,640]{1,0:T(8,128)(2,1)} %bitcast.55, bf16[2048,640]{1,0:T(8,128)(2,1)} %bitcast.56), custom_call_target="tpu_custom_call" | custom-call | tf_op jit(solution)/shard_map/pallas_call | solution.py:291
  36.4 0.0 copy-done.7
  36.4 2.4 %shard_map.221 = (bf16[4096,256]{1,0:T(8,128)(2,1)S(1)}, bf16[256,2048]{1,0:T(8,128)(2,1)S(1)}, bf16[32,128]{1,0:T(8,128)(2,1)S(1)}, bf16[32,128]{1,0:T(8,128)(2,1)S(1)}) custom-call(s32[2,8]{1,0:T(2,128)S(1)} %bitcast.53, f32[2,8]{1,0:T(2,128)S(1)} %bitcast.54, bf16[2048,256]{1,0:T(8,128)(2,1)} %refs_2_.2, bf16[2048,256]{1,0:T(8,128)(2,1)} %refs_3_.1, ...), custom_call_target="tpu_custom_call" | custom-call | tf_op jit(solution)/shard_map/pallas_call | solution.py:214
  38.8 0.0 collective-permute-done.10.refs_3_
  38.8 0.0 collective-permute-done.8.refs_1_
  38.8 0.0 collective-permute-done.9.refs_2_
  38.9 0.0 copy-done.2
  38.9 0.3 shard_map.227
  39.2 0.1 collective-permute-start.11
  39.3 1.2 %collective-permute-done.11 = bf16[16,2176]{1,0:T(8,128)(2,1)S(1)} collective-permute-done((bf16[16,2176]{1,0:T(8,128)(2,1)S(1)}, bf16[16,2176]{1,0:T(8,128)(2,1)S(1)}, u32[]{:S(2)}, u32[]{:S(2)}) %collective-permute-start.11) | collective-permute-done | bytes 69664 | tf_op jit(solution)/shard_map/ppermute | solution.py:310
  40.6 1.7 %collective-permute-start.14 = (bf16[8,2176]{1,0:T(8,128)(2,1)S(1)}, bf16[8,2176]{1,0:T(8,128)(2,1)S(1)}, u32[]{:S(2)}, u32[]{:S(2)}) collective-permute-start(bf16[8,2176]{1,0:T(8,128)(2,1)S(1)} %pad_maximum_fusion.3), channel_id=1, source_target_pairs={{0,24},{4,28},{8,16},{12,20},{16,8},{20,12},{24,0},{28,4},{1,25},{... | collective-permute-start | bytes 104456 | tf_op jit(solution)/shard_map/ppermute | solution.py:315
  42.2 0.1 collective-permute-start.13
  42.3 2.8 %collective-permute-start.12 = (bf16[8,2176]{1,0:T(8,128)(2,1)S(1)}, bf16[8,2176]{1,0:T(8,128)(2,1)S(1)}, u32[]{:S(2)}, u32[]{:S(2)}) collective-permute-start(bf16[8,2176]{1,0:T(8,128)(2,1)S(1)} %pad_maximum_fusion.1), channel_id=1, source_target_pairs={{0,8},{4,12},{8,0},{12,4},{16,24},{20,28},{24,16},{28,20},{1,9},{5... | collective-permute-start | bytes 104456 | tf_op jit(solution)/shard_map/ppermute | solution.py:315
  45.2 1.3 %collective-permute-done.14.refs_3_ = bf16[8,2176]{1,0:T(8,128)(2,1)S(1)} collective-permute-done((bf16[8,2176]{1,0:T(8,128)(2,1)S(1)}, bf16[8,2176]{1,0:T(8,128)(2,1)S(1)}, u32[]{:S(2)}, u32[]{:S(2)}) %collective-permute-start.14) | collective-permute-done | bytes 34848 | tf_op jit(solution)/shard_map/ppermute | solution.py:315
  46.5 0.9 %collective-permute-done.13.refs_2_ = bf16[8,2176]{1,0:T(8,128)(2,1)S(1)} collective-permute-done((bf16[8,2176]{1,0:T(8,128)(2,1)S(1)}, bf16[8,2176]{1,0:T(8,128)(2,1)S(1)}, u32[]{:S(2)}, u32[]{:S(2)}) %collective-permute-start.13) | collective-permute-done | bytes 34848 | tf_op jit(solution)/shard_map/ppermute | solution.py:315
  47.4 0.3 collective-permute-done.12.refs_1_
  47.8 2.7 %shard_map.229 = bf16[32,16,128]{2,1,0:T(8,128)(2,1)} custom-call(bf16[8,2176]{1,0:T(8,128)(2,1)S(1)} %pad_maximum_fusion.refs_0_, bf16[8,2176]{1,0:T(8,128)(2,1)S(1)} %collective-permute-done.12.refs_1_, bf16[8,2176]{1,0:T(8,128)(2,1)S(1)} %collective-permute-done.13.refs_2_, bf16[8,2176]{1,0:T(8,128)(2,1)S(1)} %collective-permute-done.14.refs_3_, ...), custom_call_target="tpu_custom_call" | custom-call | tf_op jit(solution)/shard_map/pallas_call | solution.py:168
  50.5 3.9 %all-to-all-start = ((bf16[32,16,128]{2,1,0:T(8,128)(2,1)}), bf16[32,16,128]{2,1,0:T(8,128)(2,1)S(1)}, u32[]{:S(2)}, u32[]{:S(2)}) async-start(bf16[32,16,128]{2,1,0:T(8,128)(2,1)} %shard_map.229), calls=%async_computation | async-start | bytes 262144 | tf_op jit(solution)/shard_map/all_to_all | solution.py:655
  54.4 0.6 slice.85
  55.0 0.7 %fusion.30 = bf16[8,1024]{1,0:T(8,128)(2,1)} fusion(f32[8,8]{0,1:T(8,128)S(1)} %add_rsqrt_fusion, bf16[8,3072]{1,0:T(8,128)(2,1)S(1)} %fusion.23), kind=kLoop, calls=%fused_computation.44 | loop fusion | flops 24576 | bytes 33024 | tf_op jit(solution)/shard_map/convert_element_type | solution.py:611
  55.7 7.1 %all-to-all-done.returned_ref = bf16[32,16,128]{2,1,0:T(8,128)(2,1)S(1)} async-done(((bf16[32,16,128]{2,1,0:T(8,128)(2,1)}), bf16[32,16,128]{2,1,0:T(8,128)(2,1)S(1)}, u32[]{:S(2)}, u32[]{:S(2)}) %all-to-all-start) | async-done | bytes 131104 | tf_op jit(solution)/shard_map/all_to_all | solution.py:655
  62.8 0.7 %shard_map.230 = bf16[8,512]{1,0:T(8,128)(2,1)} custom-call(bf16[32,512]{1,0:T(8,128)(2,1)S(1)} %shard_map.220.picks_ref, bf16[32,16,128]{2,1,0:T(8,128)(2,1)S(1)} %all-to-all-done.returned_ref, f32[8,512]{1,0:T(8,128)S(1)} %get-tuple-element.32.middle_ref), custom_call_target="tpu_custom_call" | custom-call | tf_op jit(solution)/shard_map/pallas_call | solution.py:168
  (25 shorter events, 0.2 us)
Async XLA Ops:
  0.6 1.6 %collective-permute-start = (bf16[8,2048]{1,0:T(8,128)(2,1)}, bf16[8,2048]{1,0:T(8,128)(2,1)S(1)}, u32[]{:S(2)}, u32[]{:S(2)}) collective-permute-start(bf16[8,2048]{1,0:T(8,128)(2,1)} %tokens_ref.5), channel_id=1, source_target_pairs={{0,4},{4,0},{8,12},{12,8},{16,20},{20,16},{24,28},{28,24},{1,5},{5... | collective-permute-start | bytes 98312 | tf_op jit(solution)/shard_map/ppermute | solution.py:310
  2.3 0.8 %copy-start.1 = (bf16[8,2048]{1,0:T(8,128)(2,1)S(1)}, bf16[8,2048]{1,0:T(8,128)(2,1)}, u32[]{:S(2)}) copy-start(bf16[8,2048]{1,0:T(8,128)(2,1)} %tokens_ref.5) | copy-start | bytes 98308
  3.0 11.0 %copy-start.3 = (f32[2048]{0:T(1024)S(1)}, f32[2048]{0:T(1024)}, u32[]{:S(2)}) copy-start(f32[2048]{0:T(1024)} %param.22) | copy-start | bytes 24580
  3.0 11.5 %copy-start.10 = (s32[8]{0:T(128)S(1)}, s32[8]{0:T(128)}, u32[]{:S(2)}) copy-start(s32[8]{0:T(128)} %param.30) | copy-start | bytes 100
  3.0 9.8 %collective-permute-start.1 = (bf16[16,256]{1,0:T(8,128)(2,1)S(1)}, bf16[16,256]{1,0:T(8,128)(2,1)S(1)}, u32[]{:S(2)}, u32[]{:S(2)}) collective-permute-start(bf16[16,256]{1,0:T(8,128)(2,1)S(1)} %get-tuple-element.21), channel_id=1, source_target_pairs={{0,8},{4,12},{8,0},{12,4},{16,24},{20,28},{24,16},{28,20},{1,9},{5... | collective-permute-start | bytes 24584 | tf_op jit(solution)/shard_map/ppermute | solution.py:315
  6.0 6.8 %collective-permute-start.2 = (bf16[16,256]{1,0:T(8,128)(2,1)S(1)}, bf16[16,256]{1,0:T(8,128)(2,1)S(1)}, u32[]{:S(2)}, u32[]{:S(2)}) collective-permute-start(bf16[16,256]{1,0:T(8,128)(2,1)S(1)} %get-tuple-element.22), channel_id=1, source_target_pairs={{0,16},{4,20},{8,24},{12,28},{16,0},{20,4},{24,8},{28,12},{1,17},{... | collective-permute-start | bytes 24584 | tf_op jit(solution)/shard_map/ppermute | solution.py:315
  8.6 5.4 %collective-permute-start.3 = (bf16[16,256]{1,0:T(8,128)(2,1)S(1)}, bf16[16,256]{1,0:T(8,128)(2,1)S(1)}, u32[]{:S(2)}, u32[]{:S(2)}) collective-permute-start(bf16[16,256]{1,0:T(8,128)(2,1)S(1)} %get-tuple-element.23), channel_id=1, source_target_pairs={{0,24},{4,28},{8,16},{12,20},{16,8},{20,12},{24,0},{28,4},{1,25},{... | collective-permute-start | bytes 24584 | tf_op jit(solution)/shard_map/ppermute | solution.py:315
  14.4 1.5 %collective-permute-start.4 = (bf16[32,3072]{1,0:T(8,128)(2,1)S(1)}, bf16[32,3072]{1,0:T(8,128)(2,1)S(1)}, u32[]{:S(2)}, u32[]{:S(2)}) collective-permute-start(bf16[32,3072]{1,0:T(8,128)(2,1)S(1)} %get-tuple-element.26), channel_id=1, source_target_pairs={{0,4},{4,0},{8,12},{12,8},{16,20},{20,16},{24,28},{28,24},{1,5},{5... | collective-permute-start | bytes 589832 | tf_op jit(solution)/shard_map/ppermute | solution.py:310
  16.0 8.1 %collective-permute-start.5 = (bf16[8,3072]{1,0:T(8,128)(2,1)S(1)}, bf16[8,3072]{1,0:T(8,128)(2,1)S(1)}, u32[]{:S(2)}, u32[]{:S(2)}) collective-permute-start(bf16[8,3072]{1,0:T(8,128)(2,1)S(1)} %get-tuple-element.37), channel_id=1, source_target_pairs={{0,8},{4,12},{8,0},{12,4},{16,24},{20,28},{24,16},{28,20},{1,9},{5... | collective-permute-start | bytes 147464 | tf_op jit(solution)/shard_map/ppermute | solution.py:315
  16.1 8.0 %collective-permute-start.6 = (bf16[8,3072]{1,0:T(8,128)(2,1)S(1)}, bf16[8,3072]{1,0:T(8,128)(2,1)S(1)}, u32[]{:S(2)}, u32[]{:S(2)}) collective-permute-start(bf16[8,3072]{1,0:T(8,128)(2,1)S(1)} %get-tuple-element.39), channel_id=1, source_target_pairs={{0,16},{4,20},{8,24},{12,28},{16,0},{20,4},{24,8},{28,12},{1,17},{... | collective-permute-start | bytes 147464 | tf_op jit(solution)/shard_map/ppermute | solution.py:315
  19.3 5.9 %collective-permute-start.7 = (bf16[8,3072]{1,0:T(8,128)(2,1)S(1)}, bf16[8,3072]{1,0:T(8,128)(2,1)S(1)}, u32[]{:S(2)}, u32[]{:S(2)}) collective-permute-start(bf16[8,3072]{1,0:T(8,128)(2,1)S(1)} %get-tuple-element.38), channel_id=1, source_target_pairs={{0,24},{4,28},{8,16},{12,20},{16,8},{20,12},{24,0},{28,4},{1,25},{... | collective-permute-start | bytes 147464 | tf_op jit(solution)/shard_map/ppermute | solution.py:315
  20.6 4.8 %copy-start.9 = (f32[128]{0:T(128)S(1)}, f32[128]{0:T(128)}, u32[]{:S(2)}) copy-start(f32[128]{0:T(128)} %param.26) | copy-start | bytes 1540
  24.1 2.6 %copy-start.11 = (f32[8]{0:T(128)S(1)}, f32[8]{0:T(128)}, u32[]{:S(2)}) copy-start(f32[8]{0:T(128)} %param.27) | copy-start | bytes 100
  26.7 2.2 %copy-start.8 = (bf16[1024,2048]{1,0:T(8,128)(2,1)S(1)}, bf16[1024,2048]{1,0:T(8,128)(2,1)}, u32[]{:S(2)}) copy-start(bf16[1024,2048]{1,0:T(8,128)(2,1)} %param.31) | copy-start | bytes 12582916
  26.7 6.4 %copy-start.6 = (s32[8,2]{0,1:T(2,128)S(1)}, s32[8,2]{0,1:T(2,128)}, u32[]{:S(2)}) copy-start(s32[8,2]{0,1:T(2,128)} %param.33) | copy-start | bytes 196
  28.4 7.9 %copy-start.7 = (f32[8,2]{0,1:T(2,128)S(1)}, f32[8,2]{0,1:T(2,128)}, u32[]{:S(2)}) copy-start(f32[8,2]{0,1:T(2,128)} %param.34) | copy-start | bytes 196
  28.9 10.0 %copy-start.2 = (bf16[8,2048]{1,0:T(8,128)(2,1)S(1)}, bf16[8,2048]{1,0:T(8,128)(2,1)}, u32[]{:S(2)}) copy-start(bf16[8,2048]{1,0:T(8,128)(2,1)} %tokens_ref.5) | copy-start | bytes 98308
  28.9 10.0 %copy-start.4 = (f32[2048]{0:T(1024)S(1)}, f32[2048]{0:T(1024)}, u32[]{:S(2)}) copy-start(f32[2048]{0:T(1024)} %param.32) | copy-start | bytes 24580
  28.9 18.9 %copy-start = (bf16[1,640,2048]{2,1,0:T(8,128)(2,1)S(1)}, bf16[1,640,2048]{2,1,0:T(8,128)(2,1)}, u32[]{:S(2)}) copy-start(bf16[1,640,2048]{2,1,0:T(8,128)(2,1)} %param.37) | copy-start | bytes 7864324
  28.9 18.9 %copy-start.5 = (f32[2048]{0:T(1024)S(1)}, f32[2048]{0:T(1024)}, u32[]{:S(2)}) copy-start(f32[2048]{0:T(1024)} %param.41) | copy-start | bytes 24580
  29.5 9.3 %collective-permute-start.10 = (bf16[8,2048]{1,0:T(8,128)(2,1)S(1)}, bf16[8,2048]{1,0:T(8,128)(2,1)S(1)}, u32[]{:S(2)}, u32[]{:S(2)}) collective-permute-start(bf16[8,2048]{1,0:T(8,128)(2,1)S(1)} %convolution_convert_fusion.refs_0_), channel_id=1, source_target_pairs={{0,3},{1,2},{2,1},{3,0},{4,7},{5,6},{6,5},{7,4},{8,11},{9,10},{10,... | collective-permute-start | bytes 98312 | tf_op jit(solution)/shard_map/ppermute | solution.py:320
  32.0 6.9 %collective-permute-start.8 = (bf16[8,2048]{1,0:T(8,128)(2,1)S(1)}, bf16[8,2048]{1,0:T(8,128)(2,1)S(1)}, u32[]{:S(2)}, u32[]{:S(2)}) collective-permute-start(bf16[8,2048]{1,0:T(8,128)(2,1)S(1)} %convolution_convert_fusion.refs_0_), channel_id=1, source_target_pairs={{0,1},{1,0},{2,3},{3,2},{4,5},{5,4},{6,7},{7,6},{8,9},{9,8},{10,11... | collective-permute-start | bytes 98312 | tf_op jit(solution)/shard_map/ppermute | solution.py:320
  32.5 6.3 %collective-permute-start.9 = (bf16[8,2048]{1,0:T(8,128)(2,1)S(1)}, bf16[8,2048]{1,0:T(8,128)(2,1)S(1)}, u32[]{:S(2)}, u32[]{:S(2)}) collective-permute-start(bf16[8,2048]{1,0:T(8,128)(2,1)S(1)} %convolution_convert_fusion.refs_0_), channel_id=1, source_target_pairs={{0,2},{1,3},{2,0},{3,1},{4,6},{5,7},{6,4},{7,5},{8,10},{9,11},{10,... | collective-permute-start | bytes 98312 | tf_op jit(solution)/shard_map/ppermute | solution.py:320
  39.2 1.3 %collective-permute-start.11 = (bf16[16,2176]{1,0:T(8,128)(2,1)S(1)}, bf16[16,2176]{1,0:T(8,128)(2,1)S(1)}, u32[]{:S(2)}, u32[]{:S(2)}) collective-permute-start(bf16[16,2176]{1,0:T(8,128)(2,1)S(1)} %get-tuple-element.29), channel_id=1, source_target_pairs={{0,4},{4,0},{8,12},{12,8},{16,20},{20,16},{24,28},{28,24},{1,5},{5... | collective-permute-start | bytes 208904 | tf_op jit(solution)/shard_map/ppermute | solution.py:310
  40.6 5.9 %collective-permute-start.14 = (bf16[8,2176]{1,0:T(8,128)(2,1)S(1)}, bf16[8,2176]{1,0:T(8,128)(2,1)S(1)}, u32[]{:S(2)}, u32[]{:S(2)}) collective-permute-start(bf16[8,2176]{1,0:T(8,128)(2,1)S(1)} %pad_maximum_fusion.3), channel_id=1, source_target_pairs={{0,24},{4,28},{8,16},{12,20},{16,8},{20,12},{24,0},{28,4},{1,25},{... | collective-permute-start | bytes 104456 | tf_op jit(solution)/shard_map/ppermute | solution.py:315
  42.2 5.2 %collective-permute-start.13 = (bf16[8,2176]{1,0:T(8,128)(2,1)S(1)}, bf16[8,2176]{1,0:T(8,128)(2,1)S(1)}, u32[]{:S(2)}, u32[]{:S(2)}) collective-permute-start(bf16[8,2176]{1,0:T(8,128)(2,1)S(1)} %pad_maximum_fusion.2), channel_id=1, source_target_pairs={{0,16},{4,20},{8,24},{12,28},{16,0},{20,4},{24,8},{28,12},{1,17},{... | collective-permute-start | bytes 104456 | tf_op jit(solution)/shard_map/ppermute | solution.py:315
  42.3 5.4 %collective-permute-start.12 = (bf16[8,2176]{1,0:T(8,128)(2,1)S(1)}, bf16[8,2176]{1,0:T(8,128)(2,1)S(1)}, u32[]{:S(2)}, u32[]{:S(2)}) collective-permute-start(bf16[8,2176]{1,0:T(8,128)(2,1)S(1)} %pad_maximum_fusion.1), channel_id=1, source_target_pairs={{0,8},{4,12},{8,0},{12,4},{16,24},{20,28},{24,16},{28,20},{1,9},{5... | collective-permute-start | bytes 104456 | tf_op jit(solution)/shard_map/ppermute | solution.py:315
  50.5 12.3 %all-to-all-start = ((bf16[32,16,128]{2,1,0:T(8,128)(2,1)}), bf16[32,16,128]{2,1,0:T(8,128)(2,1)S(1)}, u32[]{:S(2)}, u32[]{:S(2)}) async-start(bf16[32,16,128]{2,1,0:T(8,128)(2,1)} %shard_map.229), calls=%async_computation | async-start | bytes 262144 | tf_op jit(solution)/shard_map/all_to_all | solution.py:655

commit v4 on v3

--- a/solution.py
+++ b/solution.py
@@ -593,7 +593,10 @@
     came = pair_move(tokens)
     scales = row_scales(tokens)
     parts = knit(tokens, came)
-    parts = [parts[0]] + [far_move(parts[step], step) for step in range(1, half)]
+    moved_parts = [parts[0]]
+    for step in range(1, half):
+        moved_parts.append(far_move(parts[step], step))
+    parts = moved_parts
     turned_keys, weights = stage_keys(key_cache, query_weight, key_weight, value_weight)
     away, kept = project(parts, attn_gain, weights, 3)
     came = pair_move(away)
@@ -623,7 +626,7 @@
     log_rest = jnp.where(visible, jax.nn.log_sigmoid(-scores), 0.0)
     later = (positions[:, None] > positions[None, :]).astype(jnp.float32)
     log_between = jnp.dot(
-        log_rest.reshape(-1, cache_slots), later, precision=lax.Precision.HIGHEST
+        log_rest.reshape(-1, cache_slots), later, precision=lax.Precision.HIGH
     ).reshape(scores.shape)
     stick = jnp.where(visible, jnp.exp(jax.nn.log_sigmoid(scores) + log_between), 0.0).astype(
         jnp.bfloat16
@@ -632,7 +635,9 @@
     attended = attended.astype(jnp.bfloat16).reshape(seq_count, head_cols)
     attn_part = jnp.dot(attended, out_weight, preferred_element_type=jnp.float32)
     attn_part = attn_part.astype(jnp.bfloat16)
-    attn_parts = [attn_part] + [tp_move(attn_part, turn) for turn in range(1, tp_size)]
+    attn_parts = [attn_part]
+    for turn in range(1, tp_size):
+        attn_parts.append(tp_move(attn_part, turn))
     ids = route_ids.T
     plan_outs, plan_work = plan_sends(capacity)
     side_in, side_back, picks, notes = stage(
@@ -647,7 +652,10 @@
     kept = kept.reshape(half, capacity, -1)
     came = came.reshape(half, capacity, -1)
     parts = [jnp.concatenate([kept[step], came[step]], axis=0) for step in range(half)]
-    parts = [parts[0]] + [far_move(parts[step], step) for step in range(1, half)]
+    moved_parts = [parts[0]]
+    for step in range(1, half):
+        moved_parts.append(far_move(parts[step], step))
+    parts = moved_parts
     (gate_up,) = stage_beside((expert_gate[0], expert_up[0]))
     blocks = experts_apply(
         parts, gate_up, expert_down[0], side_in, side_back, branch_gate, capacity

time: 63.8 us -> 63.8 us (level)
  no operation moved by 1% of the time
where the time goes in v4:
time: 63.8 us; the launch traced here: 63.5 us
  starting transfers between devices  22.7 us (36%)
  Pallas kernels  17.6 us (28%)
  waiting for transfers between devices  15.5 us (24%)
  matrix products  3.47 us (5%)
  local copies, waits for them, and re-layouts  2.13 us (3%)
  other arithmetic  1.16 us (2%)
  between operations  0.94 us (1%)
    ppermute x9, starting transfers between devices, far_move(): return lax.ppermute(values, 'ep', [(i, i ^ 2 * step) for i in range(count)])  14.6 us
    all_to_all x1, waiting for transfers between devices, fast_layer(): lax.all_to_all(blocks, ('ep', 'tp'), split_axis=0, concat_axis=0, tiled=T...  7.08 us
    pallas_call x2, Pallas kernels, stage(): pl.pallas_call(kernel, out_shape=shapes + [jax.ShapeDtypeStruct(shape, dt...  5.93 us
    ppermute x9, waiting for transfers between devices, far_move(): return lax.ppermute(values, 'ep', [(i, i ^ 2 * step) for i in range(count)])  4.81 us
    pallas_call x6, Pallas kernels, call(): pl.pallas_call(kernel, out_shape=[jax.ShapeDtypeStruct(shape, dtype) for...  4.74 us
    pallas_call x1, Pallas kernels, stage_keys(): pl.pallas_call(kernel, out_shape=[pltpu.VMEM((seqs, heads, size, slots),...  4.13 us
    all_to_all x1, starting transfers between devices, fast_layer(): lax.all_to_all(blocks, ('ep', 'tp'), split_axis=0, concat_axis=0, tiled=T...  3.91 us
    ppermute x3, waiting for transfers between devices, pair_move(): return lax.ppermute(values, 'ep', [(i, i ^ 1) for i in range(count)])  3.63 us
  transfers between devices with their start and end apart: 16, of which 9 were waited for; matrix products, arithmetic and copies ran while one was open for 2% of the time, Pallas kernels for 21%

profile of v4, /device:TPU:0, one launch (start us, length us, event | category | flops | bytes accessed | tf_op | source)
XLA Modules:
  0.0 63.5 jit_solution(1335225911071041681)
XLA Ops:
  0.6 0.6 collective-permute-start
  1.2 1.1 %collective-permute-done.came_ref = bf16[8,2048]{1,0:T(8,128)(2,1)S(1)} collective-permute-done((bf16[8,2048]{1,0:T(8,128)(2,1)}, bf16[8,2048]{1,0:T(8,128)(2,1)S(1)}, u32[]{:S(2)}, u32[]{:S(2)}) %collective-permute-start) | collective-permute-done | bytes 32800 | tf_op jit(solution)/shard_map/ppermute | solution.py:310
  2.3 0.8 %copy-done.1 = bf16[8,2048]{1,0:T(8,128)(2,1)S(1)} copy-done((bf16[8,2048]{1,0:T(8,128)(2,1)S(1)}, bf16[8,2048]{1,0:T(8,128)(2,1)}, u32[]{:S(2)}) %copy-start.1) | copy-done | bytes 32792
  3.0 3.0 %collective-permute-start.1 = (bf16[16,256]{1,0:T(8,128)(2,1)S(1)}, bf16[16,256]{1,0:T(8,128)(2,1)S(1)}, u32[]{:S(2)}, u32[]{:S(2)}) collective-permute-start(bf16[16,256]{1,0:T(8,128)(2,1)S(1)} %get-tuple-element.21), channel_id=1, source_target_pairs={{0,8},{4,12},{8,0},{12,4},{16,24},{20,28},{24,16},{28,20},{1,9},{5... | collective-permute-start | bytes 24584 | tf_op jit(solution)/shard_map/ppermute | solution.py:315
  6.0 2.6 %collective-permute-start.2 = (bf16[16,256]{1,0:T(8,128)(2,1)S(1)}, bf16[16,256]{1,0:T(8,128)(2,1)S(1)}, u32[]{:S(2)}, u32[]{:S(2)}) collective-permute-start(bf16[16,256]{1,0:T(8,128)(2,1)S(1)} %get-tuple-element.22), channel_id=1, source_target_pairs={{0,16},{4,20},{8,24},{12,28},{16,0},{20,4},{24,8},{28,12},{1,17},{... | collective-permute-start | bytes 24584 | tf_op jit(solution)/shard_map/ppermute | solution.py:315
  8.6 0.0 collective-permute-start.3
  8.6 0.1 shard_map.225
  8.7 4.1 %shard_map.223 = (bf16[8,8,128,512]{3,2,1,0:T(8,128)(2,1)S(1)}, bf16[768,1024]{1,0:T(8,128)(2,1)S(1)}) custom-call(bf16[8,8,512,128]{3,2,1,0:T(8,128)(2,1)} %keys_ref.1, bf16[256,1024]{1,0:T(8,128)(2,1)} %refs_0_.2, bf16[256,1024]{1,0:T(8,128)(2,1)} %refs_1_.1, bf16[256,1024]{1,0:T(8,128)(2,1)} %refs_2_.3), custom_call_target="tpu_custom_call" | custom-call | tf_op jit(solution)/shard_map/pallas_call | solution.py:251
  12.8 0.0 collective-permute-done.1.refs_1_
  12.8 0.0 collective-permute-done.2.refs_2_
  12.9 1.2 %collective-permute-done.3.refs_3_ = bf16[16,256]{1,0:T(8,128)(2,1)S(1)} collective-permute-done((bf16[16,256]{1,0:T(8,128)(2,1)S(1)}, bf16[16,256]{1,0:T(8,128)(2,1)S(1)}, u32[]{:S(2)}, u32[]{:S(2)}) %collective-permute-start.3) | collective-permute-done | bytes 8224 | tf_op jit(solution)/shard_map/ppermute | solution.py:315
  14.1 0.0 copy-done.3
  14.1 0.4 shard_map.224
  14.4 0.1 collective-permute-start.4
  14.5 0.0 copy-done.10
  14.5 0.1 iota_compare_fusion.1
  14.6 1.3 %collective-permute-done.4 = bf16[32,3072]{1,0:T(8,128)(2,1)S(1)} collective-permute-done((bf16[32,3072]{1,0:T(8,128)(2,1)S(1)}, bf16[32,3072]{1,0:T(8,128)(2,1)S(1)}, u32[]{:S(2)}, u32[]{:S(2)}) %collective-permute-start.4) | collective-permute-done | bytes 196640 | tf_op jit(solution)/shard_map/ppermute | solution.py:310
  16.0 0.1 fusion.41
  16.0 0.1 collective-permute-start.5
  16.1 3.2 %collective-permute-start.6 = (bf16[8,3072]{1,0:T(8,128)(2,1)S(1)}, bf16[8,3072]{1,0:T(8,128)(2,1)S(1)}, u32[]{:S(2)}, u32[]{:S(2)}) collective-permute-start(bf16[8,3072]{1,0:T(8,128)(2,1)S(1)} %get-tuple-element.39), channel_id=1, source_target_pairs={{0,16},{4,20},{8,24},{12,28},{16,0},{20,4},{24,8},{28,12},{1,17},{... | collective-permute-start | bytes 147464 | tf_op jit(solution)/shard_map/ppermute | solution.py:315
  19.3 1.2 %collective-permute-start.7 = (bf16[8,3072]{1,0:T(8,128)(2,1)S(1)}, bf16[8,3072]{1,0:T(8,128)(2,1)S(1)}, u32[]{:S(2)}, u32[]{:S(2)}) collective-permute-start(bf16[8,3072]{1,0:T(8,128)(2,1)S(1)} %get-tuple-element.38), channel_id=1, source_target_pairs={{0,24},{4,28},{8,16},{12,20},{16,8},{20,12},{24,0},{28,4},{1,25},{... | collective-permute-start | bytes 147464 | tf_op jit(solution)/shard_map/ppermute | solution.py:315
  20.5 0.1 slice_reduce_fusion
  20.6 3.5 %shard_map.226 = bf16[8,8,512,128]{3,2,1,0:T(8,128)(2,1)S(1)} custom-call(bf16[8,8,512,128]{3,2,1,0:T(8,128)(2,1)} %refs_0_.3), custom_call_target="tpu_custom_call" | custom-call | tf_op jit(solution)/shard_map/pallas_call | solution.py:214
  24.1 0.0 copy-start.11
  24.1 0.0 collective-permute-done.5
  24.1 0.0 collective-permute-done.6
  24.1 1.1 %collective-permute-done.7 = bf16[8,3072]{1,0:T(8,128)(2,1)S(1)} collective-permute-done((bf16[8,3072]{1,0:T(8,128)(2,1)S(1)}, bf16[8,3072]{1,0:T(8,128)(2,1)S(1)}, u32[]{:S(2)}, u32[]{:S(2)}) %collective-permute-start.7) | collective-permute-done | bytes 49184 | tf_op jit(solution)/shard_map/ppermute | solution.py:315
  25.2 0.1 fusion.23
  25.3 0.1 fusion.29
  25.4 0.0 copy-done.9
  25.4 0.1 fusion.36
  25.5 1.2 %fusion.34 = f32[8,8,1,512]{3,2,1,0:T(1,128)S(1)} fusion(bf16[8,8,128,512]{3,2,1,0:T(8,128)(2,1)S(1)} %get-tuple-element.27, bf16[8,8,128,1]{2,0,1,3:T(8,128)(2,1)S(1)} %fusion.36), kind=kOutput, calls=%fused_computation.48 | convolution fusion | flops 8388608 | bytes 8536064 | tf_op jit(solution)/shard_map/shd,shdl->shl/dot_general | solution.py:620
  26.7 0.0 copy-done.11
  26.7 0.4 fusion.3
  27.1 1.2 %fusion.11 = f32[8,8,1,128]{3,2,1,0:T(1,128)S(1)} fusion(bf16[8,8,512,128]{3,2,1,0:T(8,128)(2,1)S(1)} %shard_map.226, bf16[8,8,512,1]{2,1,0,3:T(8,128)(2,1)S(1)} %fusion.3), kind=kOutput, calls=%fused_computation.16 | convolution fusion | flops 8388608 | bytes 8486912 | tf_op jit(solution)/shard_map/shl,shld->shd/dot_general | solution.py:634
  28.3 0.5 copy-done.8
  28.9 0.7 %convolution_convert_fusion.refs_0_ = bf16[8,2048]{1,0:T(8,128)(2,1)S(1)} fusion(bf16[1024,2048]{1,0:T(8,128)(2,1)S(1)} %copy-done.8, bf16[1,8,8,128]{3,2,1,0:T(8,128)(2,1)S(1)} %convert_bitcast_fusion), kind=kOutput, calls=%fused_computation | convolution fusion | flops 33570816 | bytes 4243456 | tf_op jit(solution)/shard_map/dot_general | solution.py:636
  29.5 2.5 %collective-permute-start.10 = (bf16[8,2048]{1,0:T(8,128)(2,1)S(1)}, bf16[8,2048]{1,0:T(8,128)(2,1)S(1)}, u32[]{:S(2)}, u32[]{:S(2)}) collective-permute-start(bf16[8,2048]{1,0:T(8,128)(2,1)S(1)} %convolution_convert_fusion.refs_0_), channel_id=1, source_target_pairs={{0,3},{1,2},{2,1},{3,0},{4,7},{5,6},{6,5},{7,4},{8,11},{9,10},{10,... | collective-permute-start | bytes 98312 | tf_op jit(solution)/shard_map/ppermute | solution.py:320
  32.0 0.5 collective-permute-start.8
  32.5 0.5 collective-permute-start.9
  33.0 0.0 copy-done.6
  33.0 0.8 %shard_map.220.picks_ref = bf16[32,512]{1,0:T(8,128)(2,1)S(1)} custom-call(s32[2,8]{1,0:T(2,128)S(1)} %bitcast.52), custom_call_target="tpu_custom_call" | custom-call | tf_op jit(solution)/shard_map/pallas_call | solution.py:168
  33.8 2.5 %shard_map.228.refs_4_ = bf16[2048,1280]{1,0:T(8,128)(2,1)S(1)} custom-call(bf16[2048,640]{1,0:T(8,128)(2,1)} %bitcast.55, bf16[2048,640]{1,0:T(8,128)(2,1)} %bitcast.56), custom_call_target="tpu_custom_call" | custom-call | tf_op jit(solution)/shard_map/pallas_call | solution.py:291
  36.4 0.0 copy-done.7
  36.4 2.4 %shard_map.221 = (bf16[4096,256]{1,0:T(8,128)(2,1)S(1)}, bf16[256,2048]{1,0:T(8,128)(2,1)S(1)}, bf16[32,128]{1,0:T(8,128)(2,1)S(1)}, bf16[32,128]{1,0:T(8,128)(2,1)S(1)}) custom-call(s32[2,8]{1,0:T(2,128)S(1)} %bitcast.53, f32[2,8]{1,0:T(2,128)S(1)} %bitcast.54, bf16[2048,256]{1,0:T(8,128)(2,1)} %refs_2_.2, bf16[2048,256]{1,0:T(8,128)(2,1)} %refs_3_.1, ...), custom_call_target="tpu_custom_call" | custom-call | tf_op jit(solution)/shard_map/pallas_call | solution.py:214
  38.8 0.0 collective-permute-done.10.refs_3_
  38.8 0.0 collective-permute-done.8.refs_1_
  38.8 0.0 collective-permute-done.9.refs_2_
  38.9 0.0 copy-done.2
  38.9 0.3 shard_map.227
  39.2 0.1 collective-permute-start.11
  39.3 1.2 %collective-permute-done.11 = bf16[16,2176]{1,0:T(8,128)(2,1)S(1)} collective-permute-done((bf16[16,2176]{1,0:T(8,128)(2,1)S(1)}, bf16[16,2176]{1,0:T(8,128)(2,1)S(1)}, u32[]{:S(2)}, u32[]{:S(2)}) %collective-permute-start.11) | collective-permute-done | bytes 69664 | tf_op jit(solution)/shard_map/ppermute | solution.py:310
  40.6 1.7 %collective-permute-start.14 = (bf16[8,2176]{1,0:T(8,128)(2,1)S(1)}, bf16[8,2176]{1,0:T(8,128)(2,1)S(1)}, u32[]{:S(2)}, u32[]{:S(2)}) collective-permute-start(bf16[8,2176]{1,0:T(8,128)(2,1)S(1)} %pad_maximum_fusion.3), channel_id=1, source_target_pairs={{0,24},{4,28},{8,16},{12,20},{16,8},{20,12},{24,0},{28,4},{1,25},{... | collective-permute-start | bytes 104456 | tf_op jit(solution)/shard_map/ppermute | solution.py:315
  42.2 0.1 collective-permute-start.13
  42.3 2.8 %collective-permute-start.12 = (bf16[8,2176]{1,0:T(8,128)(2,1)S(1)}, bf16[8,2176]{1,0:T(8,128)(2,1)S(1)}, u32[]{:S(2)}, u32[]{:S(2)}) collective-permute-start(bf16[8,2176]{1,0:T(8,128)(2,1)S(1)} %pad_maximum_fusion.1), channel_id=1, source_target_pairs={{0,8},{4,12},{8,0},{12,4},{16,24},{20,28},{24,16},{28,20},{1,9},{5... | collective-permute-start | bytes 104456 | tf_op jit(solution)/shard_map/ppermute | solution.py:315
  45.2 1.3 %collective-permute-done.14.refs_3_ = bf16[8,2176]{1,0:T(8,128)(2,1)S(1)} collective-permute-done((bf16[8,2176]{1,0:T(8,128)(2,1)S(1)}, bf16[8,2176]{1,0:T(8,128)(2,1)S(1)}, u32[]{:S(2)}, u32[]{:S(2)}) %collective-permute-start.14) | collective-permute-done | bytes 34848 | tf_op jit(solution)/shard_map/ppermute | solution.py:315
  46.5 0.9 %collective-permute-done.13.refs_2_ = bf16[8,2176]{1,0:T(8,128)(2,1)S(1)} collective-permute-done((bf16[8,2176]{1,0:T(8,128)(2,1)S(1)}, bf16[8,2176]{1,0:T(8,128)(2,1)S(1)}, u32[]{:S(2)}, u32[]{:S(2)}) %collective-permute-start.13) | collective-permute-done | bytes 34848 | tf_op jit(solution)/shard_map/ppermute | solution.py:315
  47.4 0.3 collective-permute-done.12.refs_1_
  47.8 2.7 %shard_map.229 = bf16[32,16,128]{2,1,0:T(8,128)(2,1)} custom-call(bf16[8,2176]{1,0:T(8,128)(2,1)S(1)} %pad_maximum_fusion.refs_0_, bf16[8,2176]{1,0:T(8,128)(2,1)S(1)} %collective-permute-done.12.refs_1_, bf16[8,2176]{1,0:T(8,128)(2,1)S(1)} %collective-permute-done.13.refs_2_, bf16[8,2176]{1,0:T(8,128)(2,1)S(1)} %collective-permute-done.14.refs_3_, ...), custom_call_target="tpu_custom_call" | custom-call | tf_op jit(solution)/shard_map/pallas_call | solution.py:168
  50.5 3.9 %all-to-all-start = ((bf16[32,16,128]{2,1,0:T(8,128)(2,1)}), bf16[32,16,128]{2,1,0:T(8,128)(2,1)S(1)}, u32[]{:S(2)}, u32[]{:S(2)}) async-start(bf16[32,16,128]{2,1,0:T(8,128)(2,1)} %shard_map.229), calls=%async_computation | async-start | bytes 262144 | tf_op jit(solution)/shard_map/all_to_all | solution.py:663
  54.4 0.6 slice.85
  55.0 0.7 %fusion.30 = bf16[8,1024]{1,0:T(8,128)(2,1)} fusion(f32[8,8]{0,1:T(8,128)S(1)} %add_rsqrt_fusion, bf16[8,3072]{1,0:T(8,128)(2,1)S(1)} %fusion.23), kind=kLoop, calls=%fused_computation.44 | loop fusion | flops 24576 | bytes 33024 | tf_op jit(solution)/shard_map/convert_element_type | solution.py:614
  55.7 7.1 %all-to-all-done.returned_ref = bf16[32,16,128]{2,1,0:T(8,128)(2,1)S(1)} async-done(((bf16[32,16,128]{2,1,0:T(8,128)(2,1)}), bf16[32,16,128]{2,1,0:T(8,128)(2,1)S(1)}, u32[]{:S(2)}, u32[]{:S(2)}) %all-to-all-start) | async-done | bytes 131104 | tf_op jit(solution)/shard_map/all_to_all | solution.py:663
  62.8 0.7 %shard_map.230 = bf16[8,512]{1,0:T(8,128)(2,1)} custom-call(bf16[32,512]{1,0:T(8,128)(2,1)S(1)} %shard_map.220.picks_ref, bf16[32,16,128]{2,1,0:T(8,128)(2,1)S(1)} %all-to-all-done.returned_ref, f32[8,512]{1,0:T(8,128)S(1)} %get-tuple-element.32.middle_ref), custom_call_target="tpu_custom_call" | custom-call | tf_op jit(solution)/shard_map/pallas_call | solution.py:168
  (25 shorter events, 0.2 us)
Async XLA Ops:
  0.6 1.6 %collective-permute-start = (bf16[8,2048]{1,0:T(8,128)(2,1)}, bf16[8,2048]{1,0:T(8,128)(2,1)S(1)}, u32[]{:S(2)}, u32[]{:S(2)}) collective-permute-start(bf16[8,2048]{1,0:T(8,128)(2,1)} %tokens_ref.5), channel_id=1, source_target_pairs={{0,4},{4,0},{8,12},{12,8},{16,20},{20,16},{24,28},{28,24},{1,5},{5... | collective-permute-start | bytes 98312 | tf_op jit(solution)/shard_map/ppermute | solution.py:310
  2.3 0.8 %copy-start.1 = (bf16[8,2048]{1,0:T(8,128)(2,1)S(1)}, bf16[8,2048]{1,0:T(8,128)(2,1)}, u32[]{:S(2)}) copy-start(bf16[8,2048]{1,0:T(8,128)(2,1)} %tokens_ref.5) | copy-start | bytes 98308
  3.0 11.0 %copy-start.3 = (f32[2048]{0:T(1024)S(1)}, f32[2048]{0:T(1024)}, u32[]{:S(2)}) copy-start(f32[2048]{0:T(1024)} %param.22) | copy-start | bytes 24580
  3.0 11.5 %copy-start.10 = (s32[8]{0:T(128)S(1)}, s32[8]{0:T(128)}, u32[]{:S(2)}) copy-start(s32[8]{0:T(128)} %param.30) | copy-start | bytes 100
  3.0 9.8 %collective-permute-start.1 = (bf16[16,256]{1,0:T(8,128)(2,1)S(1)}, bf16[16,256]{1,0:T(8,128)(2,1)S(1)}, u32[]{:S(2)}, u32[]{:S(2)}) collective-permute-start(bf16[16,256]{1,0:T(8,128)(2,1)S(1)} %get-tuple-element.21), channel_id=1, source_target_pairs={{0,8},{4,12},{8,0},{12,4},{16,24},{20,28},{24,16},{28,20},{1,9},{5... | collective-permute-start | bytes 24584 | tf_op jit(solution)/shard_map/ppermute | solution.py:315
  6.0 6.8 %collective-permute-start.2 = (bf16[16,256]{1,0:T(8,128)(2,1)S(1)}, bf16[16,256]{1,0:T(8,128)(2,1)S(1)}, u32[]{:S(2)}, u32[]{:S(2)}) collective-permute-start(bf16[16,256]{1,0:T(8,128)(2,1)S(1)} %get-tuple-element.22), channel_id=1, source_target_pairs={{0,16},{4,20},{8,24},{12,28},{16,0},{20,4},{24,8},{28,12},{1,17},{... | collective-permute-start | bytes 24584 | tf_op jit(solution)/shard_map/ppermute | solution.py:315
  8.6 5.4 %collective-permute-start.3 = (bf16[16,256]{1,0:T(8,128)(2,1)S(1)}, bf16[16,256]{1,0:T(8,128)(2,1)S(1)}, u32[]{:S(2)}, u32[]{:S(2)}) collective-permute-start(bf16[16,256]{1,0:T(8,128)(2,1)S(1)} %get-tuple-element.23), channel_id=1, source_target_pairs={{0,24},{4,28},{8,16},{12,20},{16,8},{20,12},{24,0},{28,4},{1,25},{... | collective-permute-start | bytes 24584 | tf_op jit(solution)/shard_map/ppermute | solution.py:315
  14.4 1.5 %collective-permute-start.4 = (bf16[32,3072]{1,0:T(8,128)(2,1)S(1)}, bf16[32,3072]{1,0:T(8,128)(2,1)S(1)}, u32[]{:S(2)}, u32[]{:S(2)}) collective-permute-start(bf16[32,3072]{1,0:T(8,128)(2,1)S(1)} %get-tuple-element.26), channel_id=1, source_target_pairs={{0,4},{4,0},{8,12},{12,8},{16,20},{20,16},{24,28},{28,24},{1,5},{5... | collective-permute-start | bytes 589832 | tf_op jit(solution)/shard_map/ppermute | solution.py:310
  16.0 8.1 %collective-permute-start.5 = (bf16[8,3072]{1,0:T(8,128)(2,1)S(1)}, bf16[8,3072]{1,0:T(8,128)(2,1)S(1)}, u32[]{:S(2)}, u32[]{:S(2)}) collective-permute-start(bf16[8,3072]{1,0:T(8,128)(2,1)S(1)} %get-tuple-element.37), channel_id=1, source_target_pairs={{0,8},{4,12},{8,0},{12,4},{16,24},{20,28},{24,16},{28,20},{1,9},{5... | collective-permute-start | bytes 147464 | tf_op jit(solution)/shard_map/ppermute | solution.py:315
  16.1 8.0 %collective-permute-start.6 = (bf16[8,3072]{1,0:T(8,128)(2,1)S(1)}, bf16[8,3072]{1,0:T(8,128)(2,1)S(1)}, u32[]{:S(2)}, u32[]{:S(2)}) collective-permute-start(bf16[8,3072]{1,0:T(8,128)(2,1)S(1)} %get-tuple-element.39), channel_id=1, source_target_pairs={{0,16},{4,20},{8,24},{12,28},{16,0},{20,4},{24,8},{28,12},{1,17},{... | collective-permute-start | bytes 147464 | tf_op jit(solution)/shard_map/ppermute | solution.py:315
  19.3 5.9 %collective-permute-start.7 = (bf16[8,3072]{1,0:T(8,128)(2,1)S(1)}, bf16[8,3072]{1,0:T(8,128)(2,1)S(1)}, u32[]{:S(2)}, u32[]{:S(2)}) collective-permute-start(bf16[8,3072]{1,0:T(8,128)(2,1)S(1)} %get-tuple-element.38), channel_id=1, source_target_pairs={{0,24},{4,28},{8,16},{12,20},{16,8},{20,12},{24,0},{28,4},{1,25},{... | collective-permute-start | bytes 147464 | tf_op jit(solution)/shard_map/ppermute | solution.py:315
  20.6 4.8 %copy-start.9 = (f32[128]{0:T(128)S(1)}, f32[128]{0:T(128)}, u32[]{:S(2)}) copy-start(f32[128]{0:T(128)} %param.26) | copy-start | bytes 1540
  24.1 2.6 %copy-start.11 = (f32[8]{0:T(128)S(1)}, f32[8]{0:T(128)}, u32[]{:S(2)}) copy-start(f32[8]{0:T(128)} %param.27) | copy-start | bytes 100
  26.7 2.2 %copy-start.8 = (bf16[1024,2048]{1,0:T(8,128)(2,1)S(1)}, bf16[1024,2048]{1,0:T(8,128)(2,1)}, u32[]{:S(2)}) copy-start(bf16[1024,2048]{1,0:T(8,128)(2,1)} %param.31) | copy-start | bytes 12582916
  26.7 6.4 %copy-start.6 = (s32[8,2]{0,1:T(2,128)S(1)}, s32[8,2]{0,1:T(2,128)}, u32[]{:S(2)}) copy-start(s32[8,2]{0,1:T(2,128)} %param.33) | copy-start | bytes 196
  28.3 8.1 %copy-start.7 = (f32[8,2]{0,1:T(2,128)S(1)}, f32[8,2]{0,1:T(2,128)}, u32[]{:S(2)}) copy-start(f32[8,2]{0,1:T(2,128)} %param.34) | copy-start | bytes 196
  28.9 10.0 %copy-start.2 = (bf16[8,2048]{1,0:T(8,128)(2,1)S(1)}, bf16[8,2048]{1,0:T(8,128)(2,1)}, u32[]{:S(2)}) copy-start(bf16[8,2048]{1,0:T(8,128)(2,1)} %tokens_ref.5) | copy-start | bytes 98308
  28.9 10.0 %copy-start.4 = (f32[2048]{0:T(1024)S(1)}, f32[2048]{0:T(1024)}, u32[]{:S(2)}) copy-start(f32[2048]{0:T(1024)} %param.32) | copy-start | bytes 24580
  28.9 18.9 %copy-start = (bf16[1,640,2048]{2,1,0:T(8,128)(2,1)S(1)}, bf16[1,640,2048]{2,1,0:T(8,128)(2,1)}, u32[]{:S(2)}) copy-start(bf16[1,640,2048]{2,1,0:T(8,128)(2,1)} %param.37) | copy-start | bytes 7864324
  28.9 18.9 %copy-start.5 = (f32[2048]{0:T(1024)S(1)}, f32[2048]{0:T(1024)}, u32[]{:S(2)}) copy-start(f32[2048]{0:T(1024)} %param.41) | copy-start | bytes 24580
  29.5 9.3 %collective-permute-start.10 = (bf16[8,2048]{1,0:T(8,128)(2,1)S(1)}, bf16[8,2048]{1,0:T(8,128)(2,1)S(1)}, u32[]{:S(2)}, u32[]{:S(2)}) collective-permute-start(bf16[8,2048]{1,0:T(8,128)(2,1)S(1)} %convolution_convert_fusion.refs_0_), channel_id=1, source_target_pairs={{0,3},{1,2},{2,1},{3,0},{4,7},{5,6},{6,5},{7,4},{8,11},{9,10},{10,... | collective-permute-start | bytes 98312 | tf_op jit(solution)/shard_map/ppermute | solution.py:320
  32.0 6.9 %collective-permute-start.8 = (bf16[8,2048]{1,0:T(8,128)(2,1)S(1)}, bf16[8,2048]{1,0:T(8,128)(2,1)S(1)}, u32[]{:S(2)}, u32[]{:S(2)}) collective-permute-start(bf16[8,2048]{1,0:T(8,128)(2,1)S(1)} %convolution_convert_fusion.refs_0_), channel_id=1, source_target_pairs={{0,1},{1,0},{2,3},{3,2},{4,5},{5,4},{6,7},{7,6},{8,9},{9,8},{10,11... | collective-permute-start | bytes 98312 | tf_op jit(solution)/shard_map/ppermute | solution.py:320
  32.5 6.3 %collective-permute-start.9 = (bf16[8,2048]{1,0:T(8,128)(2,1)S(1)}, bf16[8,2048]{1,0:T(8,128)(2,1)S(1)}, u32[]{:S(2)}, u32[]{:S(2)}) collective-permute-start(bf16[8,2048]{1,0:T(8,128)(2,1)S(1)} %convolution_convert_fusion.refs_0_), channel_id=1, source_target_pairs={{0,2},{1,3},{2,0},{3,1},{4,6},{5,7},{6,4},{7,5},{8,10},{9,11},{10,... | collective-permute-start | bytes 98312 | tf_op jit(solution)/shard_map/ppermute | solution.py:320
  39.2 1.3 %collective-permute-start.11 = (bf16[16,2176]{1,0:T(8,128)(2,1)S(1)}, bf16[16,2176]{1,0:T(8,128)(2,1)S(1)}, u32[]{:S(2)}, u32[]{:S(2)}) collective-permute-start(bf16[16,2176]{1,0:T(8,128)(2,1)S(1)} %get-tuple-element.29), channel_id=1, source_target_pairs={{0,4},{4,0},{8,12},{12,8},{16,20},{20,16},{24,28},{28,24},{1,5},{5... | collective-permute-start | bytes 208904 | tf_op jit(solution)/shard_map/ppermute | solution.py:310
  40.6 5.9 %collective-permute-start.14 = (bf16[8,2176]{1,0:T(8,128)(2,1)S(1)}, bf16[8,2176]{1,0:T(8,128)(2,1)S(1)}, u32[]{:S(2)}, u32[]{:S(2)}) collective-permute-start(bf16[8,2176]{1,0:T(8,128)(2,1)S(1)} %pad_maximum_fusion.3), channel_id=1, source_target_pairs={{0,24},{4,28},{8,16},{12,20},{16,8},{20,12},{24,0},{28,4},{1,25},{... | collective-permute-start | bytes 104456 | tf_op jit(solution)/shard_map/ppermute | solution.py:315
  42.2 5.2 %collective-permute-start.13 = (bf16[8,2176]{1,0:T(8,128)(2,1)S(1)}, bf16[8,2176]{1,0:T(8,128)(2,1)S(1)}, u32[]{:S(2)}, u32[]{:S(2)}) collective-permute-start(bf16[8,2176]{1,0:T(8,128)(2,1)S(1)} %pad_maximum_fusion.2), channel_id=1, source_target_pairs={{0,16},{4,20},{8,24},{12,28},{16,0},{20,4},{24,8},{28,12},{1,17},{... | collective-permute-start | bytes 104456 | tf_op jit(solution)/shard_map/ppermute | solution.py:315
  42.3 5.4 %collective-permute-start.12 = (bf16[8,2176]{1,0:T(8,128)(2,1)S(1)}, bf16[8,2176]{1,0:T(8,128)(2,1)S(1)}, u32[]{:S(2)}, u32[]{:S(2)}) collective-permute-start(bf16[8,2176]{1,0:T(8,128)(2,1)S(1)} %pad_maximum_fusion.1), channel_id=1, source_target_pairs={{0,8},{4,12},{8,0},{12,4},{16,24},{20,28},{24,16},{28,20},{1,9},{5... | collective-permute-start | bytes 104456 | tf_op jit(solution)/shard_map/ppermute | solution.py:315
  50.5 12.3 %all-to-all-start = ((bf16[32,16,128]{2,1,0:T(8,128)(2,1)}), bf16[32,16,128]{2,1,0:T(8,128)(2,1)S(1)}, u32[]{:S(2)}, u32[]{:S(2)}) async-start(bf16[32,16,128]{2,1,0:T(8,128)(2,1)} %shard_map.229), calls=%async_computation | async-start | bytes 262144 | tf_op jit(solution)/shard_map/all_to_all | solution.py:663
